TPU v7x, 256 devices: a whole 4x4x8 slice. The times are simulated.
256 devices in a mesh: sp: 64 (over z, x, core), tp: 4 (over y).
Axes of the slice: x: 4, y: 4, z: 8, core: 2. Of those that a mesh axis runs over, the one named last changes fastest.
Arguments:
- queries: bfloat16 [8192, 32, 128], P('sp', 'tp'), may hold values from -6 to 6
- keys: bfloat16 [8192, 8, 128], P('sp', 'tp'), may hold values from -6 to 6
- values: bfloat16 [8192, 8, 128], P('sp', 'tp'), may hold values from -6 to 6
- q_gain: float32 [128], replicated, may hold values from 0.2 to 8
- k_gain: float32 [128], replicated, may hold values from 0.2 to 8
- w_out: bfloat16 [4096, 2048], P('tp'), may hold values from -0.09375 to 0.09375
- residual: bfloat16 [8192, 2048], P(('sp', 'tp')), may hold values from -6 to 6
- gain_mix: float32 [2048], replicated, may hold values from 0.1 to 1.9
- gain_pre: float32 [2048], replicated, may hold values from 0.1 to 1.9
- routes: int32 [8192, 4], P(('sp', 'tp')), may hold values from 0 to 63, all different within a row; in each aligned block of 32 rows (0 to 31, 32 to 63, ...) at most 4 rows name the same one
- route_weights: float32 [8192, 4], P(('sp', 'tp')), may hold values from 0.1 to 1
- w_gate: bfloat16 [64, 2048, 2048], P('sp', None, 'tp'), may hold values from -0.5 to 0.5
- w_up: bfloat16 [64, 2048, 2048], P('sp', None, 'tp'), may hold values from -0.5 to 0.5
- w_down: bfloat16 [64, 2048, 2048], P('sp', 'tp'), may hold values from -0.125 to 0.125
- gain_moe: float32 [2048], replicated, may hold values from 0.1 to 1.9
Outputs:
- layer_out: bfloat16 [8192, 2048], P(('sp', 'tp'))
Inputs may be any that keep to these rules, and one draw needn't show every extreme that they name: `routes`: each row names 4 different experts. In each aligned block of 32 rows (the rows of one device) no expert is named by more than 4 rows, a bound that some block reaches.
All inputs are finite; a program needn't handle non-finite values.
Results may differ from a plain program's by a relative error of at most 0.017.
The roundings to bfloat16 on the way count: a program that leaves them out, or rounds other values in their place, can miss the bound.
Values may be sent and summed in bfloat16 or wider, within the bound.
A program may use at most 128 MiB of HBM per device.

v0:
```python
import math

import jax
import jax.numpy as jnp
from jax import lax
from jax.sharding import PartitionSpec as P

TOP = 4
GRID_W = 64


norm_eps = 1e-06
rope_theta = 10000.0
clamp_limit = 7.0
swish_alpha = 1.702


def in_one_piece(arrays, axis, dim, along):
    ends, at = ([], 0)
    for a in arrays[:-1]:
        at += a.shape[along]
        ends.append(at)
    both = jnp.concatenate(arrays, axis=along)
    return tuple(jnp.split(lax.all_gather(both, axis, axis=dim, tiled=True), ends, axis=along))


def in_blocks(value, dim, devices):
    lengths = value.shape
    pieces = value.reshape(*lengths[:dim], devices, lengths[dim] // devices, *lengths[dim + 1 :])
    return jnp.moveaxis(pieces, dim, 0)


def sum_at_owner(value, axis, dim):
    pieces = in_blocks(value, dim, lax.axis_size(axis))
    arrived = lax.all_to_all(pieces, axis, split_axis=0, concat_axis=0, tiled=True)
    return arrived.astype(jnp.float32).sum(axis=0)


def rope_tables(positions, head_size):
    row_index = (positions // GRID_W).astype(jnp.float32)
    col_index = (positions % GRID_W).astype(jnp.float32)
    freq_count = head_size // 4
    inverse = rope_theta ** (-jnp.arange(freq_count, dtype=jnp.float32) / freq_count)
    angles = jnp.stack([row_index[:, None] * inverse, col_index[:, None] * inverse], axis=1)
    return (jnp.cos(angles), jnp.sin(angles))


def turn(array_in, cosine_table, sine_table):
    token_count, head_count, head_size = array_in.shape
    split_field = array_in.reshape(token_count, head_count, 2, 2, head_size // 4)
    first_half = split_field[:, :, :, 0, :]
    second_half = split_field[:, :, :, 1, :]
    cos_wide = cosine_table[:, None]
    sin_wide = sine_table[:, None]
    turned = jnp.stack(
        [
            first_half * cos_wide - second_half * sin_wide,
            second_half * cos_wide + first_half * sin_wide,
        ],
        axis=3,
    )
    return turned.reshape(token_count, head_count, head_size)


def scale_rows(array_in, gain_vec):
    return (
        array_in
        * lax.rsqrt(jnp.mean(array_in * array_in, axis=-1, keepdims=True) + norm_eps)
        * gain_vec
    )


def slot_table(route_rows, experts, capacity):
    flat_routes = route_rows.reshape(-1)
    expert_hits = (flat_routes[:, None] == jnp.arange(experts, dtype=jnp.int32)[None, :]).astype(
        jnp.int32
    )
    slot_index = jnp.sum((jnp.cumsum(expert_hits, axis=0) - expert_hits) * expert_hits, axis=1)
    target = flat_routes * capacity + slot_index
    slot_onehot = target[:, None] == jnp.arange(experts * capacity, dtype=jnp.int32)[None, :]
    return slot_onehot.astype(jnp.bfloat16).reshape(
        route_rows.shape[0], route_rows.shape[1], experts * capacity
    )


def expert_apply(arrived_rows, w_gate, w_up, w_down):
    gate_pre = jnp.minimum(
        jnp.einsum("serd,edf->serf", arrived_rows, w_gate, preferred_element_type=jnp.float32),
        clamp_limit,
    )
    up_pre = jnp.clip(
        jnp.einsum("serd,edf->serf", arrived_rows, w_up, preferred_element_type=jnp.float32),
        -clamp_limit,
        clamp_limit,
    )
    active = (gate_pre * jax.nn.sigmoid(swish_alpha * gate_pre) * (up_pre + 1.0)).astype(
        jnp.bfloat16
    )
    partial_value = jnp.einsum("serf,efd->serd", active, w_down, preferred_element_type=jnp.float32)
    return lax.optimization_barrier(partial_value.astype(jnp.bfloat16)).astype(jnp.float32)


def send_back(finished):
    return lax.all_to_all(finished, "sp", split_axis=0, concat_axis=0, tiled=True)


def on_device(
    queries,
    keys,
    values,
    q_gain,
    k_gain,
    w_out,
    residual,
    gain_mix,
    gain_pre,
    routes,
    route_weights,
    w_gate,
    w_up,
    w_down,
    gain_moe,
):
    tok_rows, head_local, head_size = queries.shape
    kv_local = keys.shape[1]
    group_size = head_local // kv_local
    positions = lax.axis_index("sp") * tok_rows + jnp.arange(tok_rows, dtype=jnp.int32)
    cosine_table, sine_table = rope_tables(positions, head_size)
    q_turned = (
        turn(scale_rows(queries.astype(jnp.float32), q_gain), cosine_table, sine_table)
        * head_size ** (-0.5)
    ).astype(jnp.bfloat16)
    k_turned = turn(scale_rows(keys.astype(jnp.float32), k_gain), cosine_table, sine_table).astype(
        jnp.bfloat16
    )
    q_grouped = q_turned.reshape(tok_rows, kv_local, group_size, head_size)
    initial = (
        jnp.full((kv_local, group_size, tok_rows), -jnp.inf, jnp.float32),
        jnp.zeros((kv_local, group_size, tok_rows), jnp.float32),
        jnp.zeros((kv_local, group_size, tok_rows, head_size), jnp.float32),
    )
    carry_state = initial
    key_piece, value_piece = in_one_piece((k_turned, values), "sp", 0, 1)
    piece_rows = key_piece.shape[0]
    block_rows = math.gcd(piece_rows, 1024)
    key_blocks = key_piece.reshape(piece_rows // block_rows, block_rows, kv_local, head_size)
    value_blocks = value_piece.reshape(piece_rows // block_rows, block_rows, kv_local, head_size)

    def absorb_block(state_now, key_value):
        running_max, running_sum, weighted = state_now
        key_block, value_block = key_value
        scores = jnp.einsum(
            "qkgd,skd->kgqs", q_grouped, key_block, preferred_element_type=jnp.float32
        )
        new_max = jnp.maximum(running_max, jnp.max(scores, axis=-1))
        rescale = jnp.exp(running_max - new_max)
        unnorm = jnp.exp(scores - new_max[..., None])
        running_sum = running_sum * rescale + jnp.sum(unnorm, axis=-1)
        weighted = weighted * rescale[..., None] + jnp.einsum(
            "kgqs,skd->kgqd",
            unnorm.astype(jnp.bfloat16),
            value_block,
            preferred_element_type=jnp.float32,
        )
        return ((new_max, running_sum, weighted), None)

    carry_state, ignored = lax.scan(absorb_block, carry_state, (key_blocks, value_blocks))
    running_max, running_sum, weighted = carry_state
    mixed_heads = (weighted / running_sum[..., None]).transpose(2, 0, 1, 3)
    mixed_heads = mixed_heads.reshape(tok_rows, head_local * head_size).astype(jnp.bfloat16)
    tok_part = residual.shape[0]
    width = residual.shape[1]
    projected = sum_at_owner(
        jnp.dot(mixed_heads, w_out, preferred_element_type=jnp.float32).astype(jnp.bfloat16),
        "tp",
        0,
    )
    middle = residual.astype(jnp.float32) + scale_rows(projected, gain_mix)
    normed = scale_rows(middle, gain_pre).astype(jnp.bfloat16)
    local_experts = w_gate.shape[0]
    experts_all = local_experts * lax.axis_size("sp")
    capacity = max(2, (2 * tok_part * TOP + experts_all - 1) // experts_all)
    tables = slot_table(routes, experts_all, capacity)
    chosen = jnp.sum(tables, axis=1)
    outbound = jnp.einsum("tp,td->pd", chosen, normed, preferred_element_type=jnp.float32)
    outbound = outbound.astype(jnp.bfloat16).reshape(experts_all, capacity, width)
    arrived_rows = lax.all_gather(
        lax.all_to_all(outbound, "sp", split_axis=0, concat_axis=0, tiled=True),
        "tp",
        axis=0,
        tiled=True,
    )
    leading = arrived_rows.shape[0] // local_experts
    partial_value = expert_apply(
        arrived_rows.reshape(leading, local_experts, arrived_rows.shape[1], width),
        w_gate,
        w_up,
        w_down,
    )
    summed = lax.psum_scatter(
        partial_value.reshape(arrived_rows.shape).astype(jnp.bfloat16),
        "tp",
        scatter_dimension=0,
        tiled=True,
    )
    returned = send_back(summed)
    gathered = jnp.einsum(
        "tkp,pd->tkd",
        tables,
        returned.reshape(experts_all * capacity, width),
        preferred_element_type=jnp.float32,
    )
    mixture = jnp.sum(gathered * route_weights[:, :, None], axis=1)
    return (middle + scale_rows(mixture, gain_moe)).astype(jnp.bfloat16)


def solution(mesh):
    placed = (
        P("sp", "tp", None),
        P("sp", "tp", None),
        P("sp", "tp", None),
        P(),
        P(),
        P("tp", None),
        P(("sp", "tp"), None),
        P(),
        P(),
        P(("sp", "tp"), None),
        P(("sp", "tp"), None),
        P("sp", None, "tp"),
        P("sp", None, "tp"),
        P("sp", "tp", None),
        P(),
    )
    return jax.shard_map(
        on_device, mesh=mesh, in_specs=placed, out_specs=P(("sp", "tp"), None), check_vma=False
    )
```

profile of v0, /device:TPU:1, one launch (start us, length us, event | category | flops | bytes accessed | tf_op | source)
XLA Modules:
  0.0 420.4 jit_solution(8629019498525341553)
XLA Ops:
  13.2 86.5 %all-gather.3.cloned.1.call-done = bf16[8192,4,128]{0,2,1:T(8,128)(2,1)} async-done(((bf16[128,4,128]{0,2,1:T(8,128)(2,1)}), bf16[8192,4,128]{0,2,1:T(8,128)(2,1)}) %all-gather.3.cloned.1.call-update) | async-done | bytes 8388624 | tf_op jit(solution)/shard_map/all_gather | solution.py:24
  99.7 5.9 %fusion.56 = (bf16[8192,2,128]{0,2,1:T(8,128)(2,1)}, bf16[8192,2,128]{0,2,1:T(8,128)(2,1)}) fusion(bf16[8192,4,128]{0,2,1:T(8,128)(2,1)} %all-gather.3.cloned.1.call-done), kind=kLoop, calls=%fused_computation.98 | loop fusion | bytes 16777216 | tf_op jit(solution)/shard_map/split | solution.py:24
  105.6 6.4 %copy.76 = bf16[8192,2,128]{2,0,1:T(8,128)(2,1)} copy(bf16[8192,2,128]{0,2,1:T(8,128)(2,1)} %get-tuple-element.116) | data formatting | bytes 8388608 | tf_op jit(solution)/shard_map/split | solution.py:24
  112.0 6.3 %copy.78 = bf16[8192,2,128]{2,0,1:T(8,128)(2,1)} copy(bf16[8192,2,128]{0,2,1:T(8,128)(2,1)} %get-tuple-element.115) | data formatting | bytes 8388608 | tf_op jit(solution)/shard_map/split | solution.py:24
  118.3 75.6 %while.15 = (s32[]{:T(128)}, f32[2,4,128]{2,1,0:T(4,128)S(1)}, f32[2,4,128]{2,1,0:T(4,128)S(1)}, f32[2,4,128,128]{3,2,1,0:T(8,128)S(1)}, bf16[8,1024,2,128]{3,1,...) while((s32[]{:T(128)}, f32[2,4,128]{2,1,0:T(4,128)S(1)}, ...), condition=%wide.region_5.6_spmd.clone, body=%wide.region_2.5_spmd.clone.sunk | while | flops 542512128 | bytes 31786116 | solution.py:167
  118.3 3.7 bitcast_reduce_fusion.2
  122.0 2.9 fusion.73
  125.5 2.2 fusion.75
  127.7 3.7 bitcast_reduce_fusion.2
  131.5 2.9 fusion.73
  137.2 3.7 bitcast_reduce_fusion.2
  140.9 2.9 fusion.73
  146.7 3.7 bitcast_reduce_fusion.2
  150.4 2.9 fusion.73
  156.1 3.7 bitcast_reduce_fusion.2
  159.8 2.9 fusion.73
  165.6 3.7 bitcast_reduce_fusion.2
  169.3 2.9 fusion.73
  175.0 3.7 bitcast_reduce_fusion.2
  178.8 2.9 fusion.73
  184.5 3.7 bitcast_reduce_fusion.2
  188.2 2.9 fusion.73
  194.2 3.7 convolution_convert_fusion.1
  197.9 4.0 all-to-all-start
  202.4 8.5 %all-to-all-done = bf16[4,32,2048]{2,1,0:T(8,128)(2,1)S(1)} async-done(((bf16[4,32,2048]{2,1,0:T(8,128)(2,1)}), bf16[4,32,2048]{2,1,0:T(8,128)(2,1)S(1)}, u32[]{:S(2)}, u32[]{:S(2)}) %all-to-all-start) | async-done | bytes 524320 | tf_op jit(solution)/shard_map/all_to_all | solution.py:35
  212.9 2.3 reshape.304
  215.2 38.7 %all_to_all.15 = bf16[64,4,2048]{2,1,0:T(4,128)(2,1)S(1)} all-to-all(bf16[64,4,2048]{2,1,0:T(4,128)(2,1)} %reshape.304), channel_id=1, replica_groups=mesh['sp'=64,'tp'=4] {'sp'}, dimensions={0} | all-to-all | bytes 2097152 | tf_op jit(solution)/shard_map/all_to_all | solution.py:188
  255.7 45.6 %all-gather.5.cloned.1.call-done = bf16[256,4,2048]{2,0,1:T(8,128)(2,1)} async-done(((bf16[64,4,2048]{2,0,1:T(8,128)(2,1)}), bf16[256,4,2048]{2,0,1:T(8,128)(2,1)}) %all-gather.5.cloned.1.call-update) | async-done | bytes 4194320 | tf_op jit(solution)/shard_map/all_gather | solution.py:187
  301.3 6.6 %fusion.19 = f32[256,4,512]{2,0,1:T(8,128)} fusion(bf16[256,4,2048]{2,0,1:T(8,128)(2,1)} %all-gather.5.cloned.1.call-done, bf16[1,2048,512]{2,1,0:T(8,128)(2,1)} %param.29), kind=kOutput, calls=%fused_computation.27 | convolution fusion | flops 2147483648 | bytes 8388608 | tf_op jit(solution)/shard_map/serd,edf->serf/dot_general | solution.py:92
  307.9 10.3 %convert_bitcast_fusion = bf16[256,1,4,2048]{3,0,2,1:T(8,128)(2,1)} fusion(bf16[1,512,2048]{2,1,0:T(8,128)(2,1)S(1)} %copy-done, f32[256,4,512]{2,0,1:T(8,128)} %fusion.19, bf16[256,4,2048]{2,0,1:T(8,128)(2,1)} %all-gather.5.cloned.1.call-done, bf16[1,2048,512]{2,1,0:T(8,128)(2,1)} %param.28), kind=kOutput, calls=%fused_computation.20 | convolution fusion | flops 4302307328 | bytes 14680064 | tf_op jit(solution)/shard_map/serf,efd->serd/dot_general | solution.py:99
  318.3 50.0 %reduce-scatter.2.cloned.1.call-done = bf16[64,4,2048]{2,0,1:T(8,128)(2,1)} async-done(((bf16[256,4,2048]{2,0,1:T(8,128)(2,1)}), bf16[64,4,2048]{2,0,1:T(8,128)(2,1)}) %reduce-scatter.2.cloned.1.call-update) | async-done | bytes 1048592 | tf_op jit(solution)/shard_map/reduce_scatter | solution.py:200
  370.3 38.8 %all_to_all.16 = bf16[64,4,2048]{2,1,0:T(4,128)(2,1)} all-to-all(bf16[64,4,2048]{2,1,0:T(4,128)(2,1)S(1)} %copy.86), channel_id=1, replica_groups=mesh['sp'=64,'tp'=4] {'sp'}, dimensions={0} | all-to-all | bytes 2097152 | tf_op jit(solution)/shard_map/all_to_all | solution.py:104
  (113 shorter events, 37.8 us)
Async XLA Ops:
  6.5 301.4 %copy-start = (bf16[1,512,2048]{2,1,0:T(8,128)(2,1)S(1)}, bf16[1,512,2048]{2,1,0:T(8,128)(2,1)}, u32[]{:S(2)}) copy-start(bf16[1,512,2048]{2,1,0:T(8,128)(2,1)} %param.30) | copy-start | bytes 6291460
  6.5 6.2 %copy-start.6 = (s32[32,4]{0,1:T(4,128)S(1)}, s32[32,4]{0,1:T(4,128)}, u32[]{:S(2)}) copy-start(s32[32,4]{0,1:T(4,128)} %param.26) | copy-start | bytes 1540
  6.5 93.2 %all-gather.3.cloned.1.call-start = ((), (), s32[]{:S(2)}) async-start(), calls=%async_computation.4 | async-start | bytes 8519680 | tf_op jit(solution)/shard_map/all_gather | solution.py:24
  122.0 3.4 copy-start.1
  131.5 3.4 copy-start.1
  140.9 3.4 copy-start.1
  150.4 3.4 copy-start.1
  159.8 3.4 copy-start.1
  169.3 3.4 copy-start.1
  178.7 3.4 copy-start.1
  188.2 3.4 copy-start.1
  194.1 17.1 %copy-start.2 = (bf16[32,2048]{1,0:T(8,128)(2,1)S(1)}, bf16[32,2048]{1,0:T(8,128)(2,1)}, u32[]{:S(2)}) copy-start(bf16[32,2048]{1,0:T(8,128)(2,1)} %param.23) | copy-start | bytes 393220
  194.1 17.1 %copy-start.3 = (f32[2048]{0:T(1024)S(1)}, f32[2048]{0:T(1024)}, u32[]{:S(2)}) copy-start(f32[2048]{0:T(1024)} %param.24) | copy-start | bytes 24580
  194.1 17.3 %copy-start.4 = (f32[2048]{0:T(1024)S(1)}, f32[2048]{0:T(1024)}, u32[]{:S(2)}) copy-start(f32[2048]{0:T(1024)} %param.25) | copy-start | bytes 24580
  197.9 13.0 %all-to-all-start = ((bf16[4,32,2048]{2,1,0:T(8,128)(2,1)}), bf16[4,32,2048]{2,1,0:T(8,128)(2,1)S(1)}, u32[]{:S(2)}, u32[]{:S(2)}) async-start(bf16[4,32,2048]{2,1,0:T(8,128)(2,1)} %bitcast.8), calls=%async_computation | async-start | bytes 1048576 | tf_op jit(solution)/shard_map/all_to_all | solution.py:35
  201.9 99.4 %all-gather.5.cloned.1.call-start = ((), (), s32[]{:S(2)}) async-start(), calls=%async_computation.5 | async-start | bytes 5242880 | tf_op jit(solution)/shard_map/all_gather | solution.py:187
  255.5 112.8 %reduce-scatter.2.cloned.1.call-start = ((), (), s32[]{:S(2)}) async-start(), calls=%async_computation.6 | async-start | bytes 5242880 | tf_op jit(solution)/shard_map/reduce_scatter | solution.py:200
  318.2 93.1 %copy-start.7 = (f32[32,4]{0,1:T(4,128)S(1)}, f32[32,4]{0,1:T(4,128)}, u32[]{:S(2)}) copy-start(f32[32,4]{0,1:T(4,128)} %param.27) | copy-start | bytes 1540
  318.3 94.8 %copy-start.5 = (f32[2048]{0:T(1024)S(1)}, f32[2048]{0:T(1024)}, u32[]{:S(2)}) copy-start(f32[2048]{0:T(1024)} %param.31) | copy-start | bytes 24580
Sparse Core Ops, SparseCore 0:
  10.5 89.1 all-gather.2
  255.6 45.6 all-gather.4
  318.4 49.8 reduce-scatter.1
where the time goes:
time: 422 us; the launch traced here: 420 us
  waiting for transfers between devices  191 us (45%)
  blocking collectives  77.5 us (18%)
  matrix products  71.5 us (17%)
  local copies, waits for them, and re-layouts  34.8 us (8%)
  other arithmetic  28.1 us (7%)
  between operations  13.4 us (3%)
  starting transfers between devices  4.22 us (1%)
    all_gather x1, waiting for transfers between devices, in_one_piece(): lax.all_gather(both, axis, axis=dim, tiled=True)  86.5 us
    reduce_scatter x1, waiting for transfers between devices, on_device(): lax.psum_scatter(partial_value.reshape(arrived_rows.shape).astype(jnp.bfl...  50 us
    all_gather x1, waiting for transfers between devices, on_device(): lax.all_gather(lax.all_to_all(outbound, 'sp', split_axis=0, concat_axis=0...  45.6 us
    all_to_all x1, blocking collectives, send_back(): lax.all_to_all(finished, 'sp', split_axis=0, concat_axis=0, tiled=True)  38.8 us
    all_to_all x1, blocking collectives, on_device(): lax.all_to_all(outbound, 'sp', split_axis=0, concat_axis=0, tiled=True)  38.7 us
    dot_general x8, matrix products, absorb_block(): jnp.einsum('qkgd,skd->kgqs', q_grouped, key_block, preferred_element_type...  29.9 us
    reduce_sum x8, other arithmetic, absorb_block(): running_sum = running_sum * rescale + jnp.sum(unnorm, axis=-1)  23.3 us
    split x3, local copies, waits for them, and re-layouts, in_one_piece(): jnp.split(lax.all_gather(both, axis, axis=dim, tiled=True), ends, axis=al...  18.6 us
  transfers between devices with their start and end apart: 4, of which 4 were waited for; matrix products, arithmetic and copies ran while one was open for 1% of the time, Pallas kernels for 0%

commit v1 on v0

--- a/solution.py
+++ b/solution.py
@@ -1,8 +1,8 @@
-import math
-
 import jax
 import jax.numpy as jnp
 from jax import lax
+from jax.experimental import pallas as pl
+from jax.experimental.pallas import tpu as pltpu
 from jax.sharding import PartitionSpec as P
 
 TOP = 4
@@ -13,15 +13,6 @@
 rope_theta = 10000.0
 clamp_limit = 7.0
 swish_alpha = 1.702
-
-
-def in_one_piece(arrays, axis, dim, along):
-    ends, at = ([], 0)
-    for a in arrays[:-1]:
-        at += a.shape[along]
-        ends.append(at)
-    both = jnp.concatenate(arrays, axis=along)
-    return tuple(jnp.split(lax.all_gather(both, axis, axis=dim, tiled=True), ends, axis=along))
 
 
 def in_blocks(value, dim, devices):
@@ -102,6 +93,243 @@
 
 def send_back(finished):
     return lax.all_to_all(finished, "sp", split_axis=0, concat_axis=0, tiled=True)
+
+
+MESH = pl.DeviceIdType.MESH
+NZ, NX = 8, 4
+PIECE = 128
+
+
+def attention_kernel(q_ref, kv_ref, out_ref, buf, qbuf, m_ref, l_ref, acc, obuf, rsem, qsem, asem, zup, zdn, bup, bdn, bxp, bxm, bfw, dsem, osem):
+    sp = lax.axis_index("sp")
+    core = lax.rem(sp, 2)
+    chip = lax.div(sp, 2)
+    x = lax.rem(chip, NX)
+    z = lax.div(chip, NX)
+
+    def dev(zz, xx, cc):
+        return {"sp": (lax.rem(zz + 2 * NZ, NZ) * NX + lax.rem(xx + 2 * NX, NX)) * 2 + cc}
+
+    def slot(kind, zz, xx):
+        return kind * (NZ * NX) + lax.rem(zz + 2 * NZ, NZ) * NX + lax.rem(xx + 2 * NX, NX)
+
+    partner = dev(z, x, 1 - core)
+    z_up, z_dn = dev(z + 1, x, core), dev(z - 1, x, core)
+    x_up, x_dn, x_far = dev(z, x + 1, core), dev(z, x - 1, core), dev(z, x + 2, core)
+
+    mine = core * (NZ * NX) + chip
+    buf[mine] = kv_ref[core]
+    qbuf[pl.ds(pl.multiple_of(core * 512, 512), 512), :] = q_ref[core]
+    m_ref[...] = jnp.full(m_ref.shape, -jnp.inf, jnp.float32)
+    l_ref[...] = jnp.zeros(l_ref.shape, jnp.float32)
+    acc[...] = jnp.zeros(acc.shape, jnp.float32)
+
+    barrier = pltpu.get_barrier_semaphore()
+    for peer in (partner, z_up, z_dn, x_up, x_dn, x_far):
+        pl.semaphore_signal(barrier, inc=1, device_id=peer, device_id_type=MESH)
+    pl.semaphore_wait(barrier, 6)
+
+    def move(at, sem, to):
+        return pltpu.make_async_remote_copy(
+            src_ref=buf.at[at], dst_ref=buf.at[at], send_sem=sem, recv_sem=rsem.at[at], device_id=to, device_id_type=MESH
+        )
+
+    def send(at, sem, to):
+        move(at, sem, to).start()
+
+    def arrive(at):
+        move(at, dsem.at[0], partner).wait_recv()
+
+    def done(sem):
+        move(0, sem, partner).wait_send()
+
+    swap_kv = pltpu.make_async_remote_copy(
+        src_ref=kv_ref.at[1 - core], dst_ref=buf.at[(1 - core) * 0 + core * (NZ * NX) + chip], send_sem=dsem.at[0],
+        recv_sem=rsem.at[core * (NZ * NX) + chip], device_id=partner, device_id_type=MESH,
+    )
+    swap_q = pltpu.make_async_remote_copy(
+        src_ref=q_ref.at[1 - core], dst_ref=qbuf.at[pl.ds(pl.multiple_of(core * 512, 512), 512), :], send_sem=dsem.at[1],
+        recv_sem=qsem, device_id=partner, device_id_type=MESH,
+    )
+    swap_kv.start()
+    swap_q.start()
+    arrive((1 - core) * (NZ * NX) + chip)
+
+    def attend(slots):
+        keys = jnp.concatenate([buf[s, 0] for s in slots], axis=0)
+        vals = jnp.concatenate([buf[s, 1] for s in slots], axis=1)
+        for tile in range(4):
+            cols = slice(tile * 256, tile * 256 + 256)
+            scores = lax.dot_general(keys, qbuf[cols, :], (((1,), (1,)), ((), ())), preferred_element_type=jnp.float32)
+            before = m_ref[:, cols]
+            now = jnp.maximum(before, jnp.max(scores, axis=0, keepdims=True))
+            shrink = jnp.exp(before - now)
+            unnorm = jnp.exp(scores - now)
+            l_ref[:, cols] = l_ref[:, cols] * shrink + jnp.sum(unnorm, axis=0, keepdims=True)
+            acc[:, cols] = acc[:, cols] * shrink + jnp.dot(
+                vals, unnorm.astype(jnp.bfloat16), preferred_element_type=jnp.float32
+            )
+            m_ref[:, cols] = now
+
+    A, B = 0, 1
+    own_a, own_b = slot(A, z, x), slot(B, z, x)
+    send(own_b, bup.at[0], z_up)
+    send(own_b, bdn.at[0], z_dn)
+    send(own_a, asem.at[0], x_up)
+    send(own_a, asem.at[1], x_dn)
+    send(own_a, asem.at[2], x_far)
+    send(own_a, zup.at[0], z_up)
+    send(own_a, zdn.at[0], z_dn)
+    send(own_b, bxp.at[0], x_up)
+    send(own_b, bxm.at[0], x_dn)
+    for j in (1, 3, 2):
+        at = slot(A, z, x + j)
+        arrive(at)
+        send(at, zup.at[j], z_up)
+        send(at, zdn.at[j], z_dn)
+    swap_q.wait_recv()
+    attend([own_a, own_b, slot(A, z, x + 1), slot(A, z, x + 3)])
+    left, right, far = slot(B, z, x - 1), slot(B, z, x + 1), slot(B, z, x + 2)
+    arrive(right)
+    send(right, bfw.at[0], x_dn)
+    arrive(left)
+
+    def step(r, last):
+        lo, hi = z - r, z + r
+        b_lo, b_hi = slot(B, lo, x), slot(B, hi, x)
+        arrive(b_lo)
+        send(b_lo, bup.at[r], z_up)
+        send(b_lo, bxp.at[2 * r - 1], x_up)
+        send(b_lo, bxm.at[2 * r - 1], x_dn)
+        arrive(b_hi)
+
+        @pl.when(r < 3)
+        def _():
+            send(b_hi, bdn.at[r], z_dn)
+
+        send(b_hi, bxp.at[2 * r], x_up)
+        send(b_hi, bxm.at[2 * r], x_dn)
+        for pair in ((0, 1), (3, 2)):
+            group = []
+            for j in pair:
+                a_lo, a_hi = slot(A, lo, x + j), slot(A, hi, x + j)
+                group += [a_lo, a_hi]
+                arrive(a_lo)
+                if j in (0, 1):
+                    send(a_lo, zup.at[r * 4 + j], z_up)
+                else:
+                    pl.when(r < 3)(lambda a_lo=a_lo, j=j: send(a_lo, zup.at[r * 4 + j], z_up))
+                arrive(a_hi)
+                if j in (2, 3):
+                    send(a_hi, zdn.at[r * 4 + j], z_dn)
+                else:
+                    pl.when(r < 3)(lambda a_hi=a_hi, j=j: send(a_hi, zdn.at[r * 4 + j], z_dn))
+            attend(group)
+        lo_left, lo_right, lo_far = slot(B, lo, x - 1), slot(B, lo, x + 1), slot(B, lo, x + 2)
+        hi_left, hi_right, hi_far = slot(B, hi, x - 1), slot(B, hi, x + 1), slot(B, hi, x + 2)
+        arrive(lo_left)
+        send(lo_left, bfw.at[2 * r - 1], x_up)
+        arrive(hi_right)
+        send(hi_right, bfw.at[2 * r], x_dn)
+        attend([b_lo, b_hi, lo_left, hi_right])
+        arrive(lo_right)
+        arrive(hi_left)
+        arrive(lo_far)
+        arrive(hi_far)
+        attend([lo_right, hi_left, lo_far, hi_far])
+
+    arrive(far)
+    attend([slot(A, z, x + 2), left, right, far])
+
+    @pl.loop(1, 4)
+    def _(r):
+        step(r, False)
+
+    opp = z + 4
+    b_op = slot(B, opp, x)
+    arrive(b_op)
+    send(b_op, bxp.at[7], x_up)
+    send(b_op, bxm.at[7], x_dn)
+    group = []
+    for j in (0, 1, 3, 2):
+        at = slot(A, opp, x + j)
+        arrive(at)
+        group.append(at)
+    b_left, b_right, b_far = slot(B, opp, x - 1), slot(B, opp, x + 1), slot(B, opp, x + 2)
+    arrive(b_left)
+    send(b_left, bfw.at[7], x_up)
+    attend(group)
+    arrive(b_right)
+    arrive(b_far)
+    attend([b_op, b_left, b_right, b_far])
+
+    def heads_of(which):
+        cols = pl.ds(pl.multiple_of(which * 512, 512), 512)
+        return (acc[:, cols] / l_ref[:, cols]).astype(jnp.bfloat16)
+
+    theirs = heads_of(1 - core)
+    obuf[2] = theirs
+    own = heads_of(core)
+    obuf[core] = own
+    swap_o = pltpu.make_async_remote_copy(
+        src_ref=obuf.at[2], dst_ref=obuf.at[core], send_sem=osem.at[0], recv_sem=osem.at[1], device_id=partner, device_id_type=MESH
+    )
+    swap_o.start()
+    for i in range(3):
+        done(asem.at[i])
+    for i in range(4):
+        done(bup.at[i])
+        for j in range(4):
+            if i < 3 or j in (0, 1):
+                done(zup.at[i * 4 + j])
+            if i < 3 or j in (2, 3):
+                done(zdn.at[i * 4 + j])
+    for i in range(3):
+        done(bdn.at[i])
+    for i in range(8):
+        done(bxp.at[i])
+        done(bxm.at[i])
+        done(bfw.at[i])
+    swap_kv.wait_send()
+    swap_q.wait_send()
+    swap_o.wait_send()
+    swap_o.wait_recv()
+    for g in range(2):
+        for h in range(4):
+            head = obuf[g, :, h * 128 : h * 128 + 128]
+            out_ref[:, (g * 4 + h) * 128 : (g * 4 + h) * 128 + 128] = head.T
+
+
+def attention(q_two, kv_two):
+    return pl.pallas_call(
+        attention_kernel,
+        out_shape=jax.ShapeDtypeStruct((128, 1024), jnp.bfloat16),
+        in_specs=[pl.BlockSpec(memory_space=pltpu.VMEM)] * 2,
+        out_specs=pl.BlockSpec(memory_space=pltpu.VMEM),
+        scratch_shapes=[
+            pltpu.VMEM((64, 2, PIECE, 128), jnp.bfloat16),
+            pltpu.VMEM((1024, 128), jnp.bfloat16),
+            pltpu.VMEM((1, 1024), jnp.float32),
+            pltpu.VMEM((1, 1024), jnp.float32),
+            pltpu.VMEM((128, 1024), jnp.float32),
+            pltpu.VMEM((3, 128, 512), jnp.bfloat16),
+            pltpu.SemaphoreType.DMA((64,)),
+            pltpu.SemaphoreType.DMA,
+            pltpu.SemaphoreType.DMA((3,)),
+            pltpu.SemaphoreType.DMA((16,)),
+            pltpu.SemaphoreType.DMA((16,)),
+            pltpu.SemaphoreType.DMA((4,)),
+            pltpu.SemaphoreType.DMA((4,)),
+            pltpu.SemaphoreType.DMA((8,)),
+            pltpu.SemaphoreType.DMA((8,)),
+            pltpu.SemaphoreType.DMA((8,)),
+            pltpu.SemaphoreType.DMA((2,)),
+            pltpu.SemaphoreType.DMA((2,)),
+        ],
+        compiler_params=pltpu.CompilerParams(collective_id=0, has_side_effects=True),
+        cost_estimate=pl.CostEstimate(flops=4 * 1024 * 8192 * 128, bytes_accessed=1 << 20, transcendentals=1024 * 8192),
+        name="gather_attention",
+    )(q_two, kv_two)
 
 
 def on_device(
@@ -133,41 +361,9 @@
     k_turned = turn(scale_rows(keys.astype(jnp.float32), k_gain), cosine_table, sine_table).astype(
         jnp.bfloat16
     )
-    q_grouped = q_turned.reshape(tok_rows, kv_local, group_size, head_size)
-    initial = (
-        jnp.full((kv_local, group_size, tok_rows), -jnp.inf, jnp.float32),
-        jnp.zeros((kv_local, group_size, tok_rows), jnp.float32),
-        jnp.zeros((kv_local, group_size, tok_rows, head_size), jnp.float32),
-    )
-    carry_state = initial
-    key_piece, value_piece = in_one_piece((k_turned, values), "sp", 0, 1)
-    piece_rows = key_piece.shape[0]
-    block_rows = math.gcd(piece_rows, 1024)
-    key_blocks = key_piece.reshape(piece_rows // block_rows, block_rows, kv_local, head_size)
-    value_blocks = value_piece.reshape(piece_rows // block_rows, block_rows, kv_local, head_size)
-
-    def absorb_block(state_now, key_value):
-        running_max, running_sum, weighted = state_now
-        key_block, value_block = key_value
-        scores = jnp.einsum(
-            "qkgd,skd->kgqs", q_grouped, key_block, preferred_element_type=jnp.float32
-        )
-        new_max = jnp.maximum(running_max, jnp.max(scores, axis=-1))
-        rescale = jnp.exp(running_max - new_max)
-        unnorm = jnp.exp(scores - new_max[..., None])
-        running_sum = running_sum * rescale + jnp.sum(unnorm, axis=-1)
-        weighted = weighted * rescale[..., None] + jnp.einsum(
-            "kgqs,skd->kgqd",
-            unnorm.astype(jnp.bfloat16),
-            value_block,
-            preferred_element_type=jnp.float32,
-        )
-        return ((new_max, running_sum, weighted), None)
-
-    carry_state, ignored = lax.scan(absorb_block, carry_state, (key_blocks, value_blocks))
-    running_max, running_sum, weighted = carry_state
-    mixed_heads = (weighted / running_sum[..., None]).transpose(2, 0, 1, 3)
-    mixed_heads = mixed_heads.reshape(tok_rows, head_local * head_size).astype(jnp.bfloat16)
+    q_two = q_turned.transpose(1, 0, 2).reshape(kv_local, group_size * tok_rows, head_size)
+    kv_two = jnp.stack([k_turned.transpose(1, 0, 2), values.transpose(1, 2, 0)], axis=1)
+    mixed_heads = attention(q_two, kv_two)
     tok_part = residual.shape[0]
     width = residual.shape[1]
     projected = sum_at_owner(

time: 422 us -> 300 us (0.71)
  waiting for transfers between devices: 191 us -> 103 us
  Pallas kernels: 0 us -> 64.5 us
  matrix products: 71.5 us -> 23 us
  local copies, waits for them, and re-layouts: 34.8 us -> 10.7 us
  other arithmetic: 28.1 us -> 5.92 us
    all_gather x1 -> x0, waiting for transfers between devices: 86.5 us -> none  [in_one_piece(): lax.all_gather(both, axis, axis=dim, tiled=True)]
    pallas_call x0 -> x1, Pallas kernels: none -> 64.5 us  [attention(): pl.pallas_call(attention_kernel, out_shape=jax.ShapeDtypeStruct((128, 102...]
    dot_general x16 -> x0, matrix products: 47.8 us -> none  [the longest x8 29.9 us: absorb_block(): jnp.einsum('qkgd,skd->kgqs', q_grouped, key_block, preferred_element_type...]
    reduce_sum x8 -> x0, other arithmetic: 23.3 us -> none  [absorb_block(): running_sum = running_sum * rescale + jnp.sum(unnorm, axis=-1)]
    split x3 -> x0, local copies, waits for them, and re-layouts: 18.6 us -> none  [in_one_piece(): jnp.split(lax.all_gather(both, axis, axis=dim, tiled=True), ends, axis=al...]
    while x25 -> x0, local copies, waits for them, and re-layouts: 4.31 us -> none
  transfers between devices with their start and end apart: 4 -> 3, of which waited for: 4 -> 3; matrix products, arithmetic and copies ran while one was open for 1% -> 1% of each run, Pallas kernels for 0% -> 0%
where the time goes in v1:
time: 300 us; the launch traced here: 299 us
  waiting for transfers between devices  103 us (34%)
  blocking collectives  73.9 us (25%)
  Pallas kernels  64.5 us (22%)
  matrix products  23 us (8%)
  between operations  13.6 us (5%)
  local copies, waits for them, and re-layouts  10.7 us (4%)
  other arithmetic  5.92 us (2%)
  starting transfers between devices  4.36 us (1%)
    pallas_call x1, Pallas kernels, attention(): pl.pallas_call(attention_kernel, out_shape=jax.ShapeDtypeStruct((128, 102...  64.5 us
    reduce_scatter x1, waiting for transfers between devices, on_device(): lax.psum_scatter(partial_value.reshape(arrived_rows.shape).astype(jnp.bfl...  50 us
    all_gather x1, waiting for transfers between devices, on_device(): lax.all_gather(lax.all_to_all(outbound, 'sp', split_axis=0, concat_axis=0...  45.8 us
    all_to_all x1, blocking collectives, send_back(): lax.all_to_all(finished, 'sp', split_axis=0, concat_axis=0, tiled=True)  38.8 us
    all_to_all x1, blocking collectives, on_device(): lax.all_to_all(outbound, 'sp', split_axis=0, concat_axis=0, tiled=True)  35.1 us
    dot_general x1, matrix products, expert_apply(): jnp.einsum('serf,efd->serd', active, w_down, preferred_element_type=jnp.f...  10.3 us
    all_to_all x1, waiting for transfers between devices, sum_at_owner(): lax.all_to_all(pieces, axis, split_axis=0, concat_axis=0, tiled=True)  7.59 us
    dot_general x1, matrix products, expert_apply(): jnp.einsum('serd,edf->serf', arrived_rows, w_up, preferred_element_type=j...  6.59 us
  transfers between devices with their start and end apart: 3, of which 3 were waited for; matrix products, arithmetic and copies ran while one was open for 1% of the time, Pallas kernels for 0%

profile of v1, /device:TPU:1, one launch (start us, length us, event | category | flops | bytes accessed | tf_op | source)
XLA Modules:
  0.0 299.3 jit_solution(10897409705077422798)
XLA Ops:
  6.6 1.1 copy.61
  7.8 0.1 fusion.32
  7.9 0.7 fusion.22
  8.7 0.1 copy.62
  8.9 1.0 copy.63
  9.8 1.2 copy.59
  11.1 0.8 fusion.19
  12.0 0.8 copy.60
  12.8 0.7 pad_maximum_fusion.kv_ref
  13.5 64.5 %gather_attention.1 = bf16[128,1024]{1,0:T(8,128)(2,1)} custom-call(bf16[2,512,128]{2,1,0:T(8,128)(2,1)} %bitcast.91, bf16[2,2,128,128]{3,2,1,0:T(8,128)(2,1)} %pad_maximum_fusion.kv_ref), custom_call_target="tpu_custom_call" | custom-call | flops 4294967296 | bytes 1048576 | tf_op jit(solution)/shard_map/gather_attention/pallas_call | solution.py:304
  78.0 3.8 %convolution_convert_fusion.1 = bf16[128,2048]{1,0:T(8,128)(2,1)} fusion(bf16[128,1024]{1,0:T(8,128)(2,1)} %gather_attention.1, bf16[1024,2048]{1,0:T(8,128)(2,1)} %param.20), kind=kOutput, calls=%fused_computation.3 | convolution fusion | flops 537133056 | bytes 4980736 | tf_op jit(solution)/shard_map/dot_general | solution.py:370
  81.8 4.3 %all-to-all-start = ((bf16[4,32,2048]{2,1,0:T(8,128)(2,1)}), bf16[4,32,2048]{2,1,0:T(8,128)(2,1)S(1)}, u32[]{:S(2)}, u32[]{:S(2)}) async-start(bf16[4,32,2048]{2,1,0:T(8,128)(2,1)} %bitcast.10), calls=%async_computation | async-start | bytes 1048576 | tf_op jit(solution)/shard_map/all_to_all | solution.py:26
  86.4 0.2 reduce_window_sum.11
  86.6 0.2 select_reduce_fusion
  87.0 0.7 fusion.28
  87.7 7.6 %all-to-all-done = bf16[4,32,2048]{2,1,0:T(8,128)(2,1)S(1)} async-done(((bf16[4,32,2048]{2,1,0:T(8,128)(2,1)}), bf16[4,32,2048]{2,1,0:T(8,128)(2,1)S(1)}, u32[]{:S(2)}, u32[]{:S(2)}) %all-to-all-start) | async-done | bytes 524320 | tf_op jit(solution)/shard_map/all_to_all | solution.py:26
  95.4 0.1 multiply_reduce_fusion.2
  95.5 0.2 multiply_reduce_fusion.1
  95.8 1.2 convolution_convert_fusion
  97.0 1.2 reshape.293
  98.2 35.1 %all_to_all.15 = bf16[64,4,2048]{2,1,0:T(4,128)(2,1)S(1)} all-to-all(bf16[64,4,2048]{2,1,0:T(4,128)(2,1)} %reshape.293), channel_id=1, replica_groups=mesh['sp'=64,'tp'=4] {'sp'}, dimensions={0} | all-to-all | bytes 2097152 | tf_op jit(solution)/shard_map/all_to_all | solution.py:384
  133.3 1.6 copy.66
  134.9 45.8 %all-gather.2.cloned.1.call-done = bf16[256,4,2048]{2,0,1:T(8,128)(2,1)} async-done(((bf16[64,4,2048]{2,0,1:T(8,128)(2,1)}), bf16[256,4,2048]{2,0,1:T(8,128)(2,1)}) %all-gather.2.cloned.1.call-update) | async-done | bytes 4194320 | tf_op jit(solution)/shard_map/all_gather | solution.py:383
  180.7 6.6 %fusion.2 = f32[256,4,512]{2,0,1:T(8,128)} fusion(bf16[256,4,2048]{2,0,1:T(8,128)(2,1)} %all-gather.2.cloned.1.call-done, bf16[1,2048,512]{2,1,0:T(8,128)(2,1)} %param.27), kind=kOutput, calls=%fused_computation.7 | convolution fusion | flops 2147483648 | bytes 8388608 | tf_op jit(solution)/shard_map/serd,edf->serf/dot_general | solution.py:83
  187.3 10.3 %convert_bitcast_fusion = bf16[256,1,4,2048]{3,0,2,1:T(8,128)(2,1)} fusion(bf16[1,512,2048]{2,1,0:T(8,128)(2,1)S(1)} %copy-done, f32[256,4,512]{2,0,1:T(8,128)} %fusion.2, bf16[256,4,2048]{2,0,1:T(8,128)(2,1)} %all-gather.2.cloned.1.call-done, bf16[1,2048,512]{2,1,0:T(8,128)(2,1)} %param.26), kind=kOutput, calls=%fused_computation | convolution fusion | flops 4302307328 | bytes 14680064 | tf_op jit(solution)/shard_map/serf,efd->serd/dot_general | solution.py:90
  197.6 50.0 %reduce-scatter.2.cloned.1.call-done = bf16[64,4,2048]{2,0,1:T(8,128)(2,1)} async-done(((bf16[256,4,2048]{2,0,1:T(8,128)(2,1)}), bf16[64,4,2048]{2,0,1:T(8,128)(2,1)}) %reduce-scatter.2.cloned.1.call-update) | async-done | bytes 1048592 | tf_op jit(solution)/shard_map/reduce_scatter | solution.py:396
  247.7 2.0 copy.67
  249.7 38.8 %all_to_all.16 = bf16[64,4,2048]{2,1,0:T(4,128)(2,1)} all-to-all(bf16[64,4,2048]{2,1,0:T(4,128)(2,1)S(1)} %copy.67), channel_id=1, replica_groups=mesh['sp'=64,'tp'=4] {'sp'}, dimensions={0} | all-to-all | bytes 2097152 | tf_op jit(solution)/shard_map/all_to_all | solution.py:95
  288.5 1.3 reshape.302
  289.8 1.0 fusion.15
  290.9 0.1 multiply_reduce_fusion
  291.0 1.5 add_convert_fusion
  (33 shorter events, 1.1 us)
Async XLA Ops:
  6.5 180.8 %copy-start = (bf16[1,512,2048]{2,1,0:T(8,128)(2,1)S(1)}, bf16[1,512,2048]{2,1,0:T(8,128)(2,1)}, u32[]{:S(2)}) copy-start(bf16[1,512,2048]{2,1,0:T(8,128)(2,1)} %param.28) | copy-start | bytes 6291460
  78.0 8.1 %copy-start.3 = (s32[32,4]{0,1:T(4,128)S(1)}, s32[32,4]{0,1:T(4,128)}, u32[]{:S(2)}) copy-start(s32[32,4]{0,1:T(4,128)} %param.24) | copy-start | bytes 1540
  81.8 13.7 %copy-start.1 = (bf16[32,2048]{1,0:T(8,128)(2,1)S(1)}, bf16[32,2048]{1,0:T(8,128)(2,1)}, u32[]{:S(2)}) copy-start(bf16[32,2048]{1,0:T(8,128)(2,1)} %param.21) | copy-start | bytes 393220
  81.8 13.7 %copy-start.2 = (f32[2048]{0:T(1024)S(1)}, f32[2048]{0:T(1024)}, u32[]{:S(2)}) copy-start(f32[2048]{0:T(1024)} %param.22) | copy-start | bytes 24580
  81.8 13.5 %all-to-all-start = ((bf16[4,32,2048]{2,1,0:T(8,128)(2,1)}), bf16[4,32,2048]{2,1,0:T(8,128)(2,1)S(1)}, u32[]{:S(2)}, u32[]{:S(2)}) async-start(bf16[4,32,2048]{2,1,0:T(8,128)(2,1)} %bitcast.10), calls=%async_computation | async-start | bytes 1048576 | tf_op jit(solution)/shard_map/all_to_all | solution.py:26
  86.1 94.6 %all-gather.2.cloned.1.call-start = ((), (), s32[]{:S(2)}) async-start(), calls=%async_computation.4 | async-start | bytes 5242880 | tf_op jit(solution)/shard_map/all_gather | solution.py:383
  134.9 112.8 %reduce-scatter.2.cloned.1.call-start = ((), (), s32[]{:S(2)}) async-start(), calls=%async_computation.5 | async-start | bytes 5242880 | tf_op jit(solution)/shard_map/reduce_scatter | solution.py:396
Sparse Core Ops, SparseCore 0:
  135.0 45.6 all-gather.1
  197.8 49.8 reduce-scatter.1

commit v2 on v1

--- a/solution.py
+++ b/solution.py
@@ -61,38 +61,26 @@
     )
 
 
-def slot_table(route_rows, experts, capacity):
-    flat_routes = route_rows.reshape(-1)
-    expert_hits = (flat_routes[:, None] == jnp.arange(experts, dtype=jnp.int32)[None, :]).astype(
-        jnp.int32
-    )
-    slot_index = jnp.sum((jnp.cumsum(expert_hits, axis=0) - expert_hits) * expert_hits, axis=1)
-    target = flat_routes * capacity + slot_index
-    slot_onehot = target[:, None] == jnp.arange(experts * capacity, dtype=jnp.int32)[None, :]
-    return slot_onehot.astype(jnp.bfloat16).reshape(
-        route_rows.shape[0], route_rows.shape[1], experts * capacity
-    )
-
-
-def expert_apply(arrived_rows, w_gate, w_up, w_down):
-    gate_pre = jnp.minimum(
-        jnp.einsum("serd,edf->serf", arrived_rows, w_gate, preferred_element_type=jnp.float32),
-        clamp_limit,
-    )
-    up_pre = jnp.clip(
-        jnp.einsum("serd,edf->serf", arrived_rows, w_up, preferred_element_type=jnp.float32),
-        -clamp_limit,
-        clamp_limit,
-    )
-    active = (gate_pre * jax.nn.sigmoid(swish_alpha * gate_pre) * (up_pre + 1.0)).astype(
-        jnp.bfloat16
-    )
-    partial_value = jnp.einsum("serf,efd->serd", active, w_down, preferred_element_type=jnp.float32)
-    return lax.optimization_barrier(partial_value.astype(jnp.bfloat16)).astype(jnp.float32)
-
-
-def send_back(finished):
-    return lax.all_to_all(finished, "sp", split_axis=0, concat_axis=0, tiled=True)
+def slot_tables(routes, route_weights):
+    core = lax.rem(lax.axis_index("sp"), 2)
+    swap = [(i, i ^ 1) for i in range(lax.axis_size("sp"))]
+    count = routes.shape[0]
+    both = jnp.concatenate([routes.astype(jnp.float32), route_weights], axis=1)
+    other = lax.ppermute(both, "sp", swap)
+    ordered = jnp.where(core == 0, jnp.stack([both, other]), jnp.stack([other, both]))
+    chosen, weights = ordered[:, :, :TOP].astype(jnp.int32), ordered[:, :, TOP:]
+    flat = chosen.reshape(2, count * TOP)
+    same = (flat[:, :, None] == flat[:, None, :]).astype(jnp.int32)
+    place = jnp.arange(count * TOP, dtype=jnp.int32)
+    earlier = (place[None, :] < place[:, None]).astype(jnp.int32)
+    rank = jnp.sum(same * earlier, axis=2).reshape(2, count, TOP)
+    side = jnp.arange(2, dtype=jnp.int32)[:, None, None]
+    target = jnp.where(chosen % 2 == core, (chosen // 2) * 8 + side * 4 + rank, -1)
+    target, weights = target.reshape(2 * count, TOP), weights.reshape(2 * count, TOP)
+    spots = jnp.arange(256, dtype=jnp.int32)
+    disp = jnp.sum((target[None, :, :] == spots[:, None, None]).astype(jnp.float32), axis=2)
+    mixw = jnp.sum(jnp.where(target[:, None, :] == spots[None, :, None], weights[:, None, :], 0.0), axis=2)
+    return disp.astype(jnp.bfloat16), mixw
 
 
 MESH = pl.DeviceIdType.MESH
@@ -332,6 +320,232 @@
     )(q_two, kv_two)
 
 
+GROUP_ORDER = (0, 1, 7, 2, 6, 3, 5, 4)
+VIA_UP = (3, 6, 1, 0)
+VIA_DN = (4, 5, 2, 7)
+
+
+def experts_kernel(normed_ref, disp_ref, mixw_ref, middle_ref, gain_ref, wg_hbm, wu_hbm, wd_hbm, out_ref,
+                   both, msgs, rows, act, part, mid, fin, ret, mixs, wg, wu, wd,
+                   wsem, msend, mrecv, gup, gdn, gfw, grecv, s_first, s_direct, s_mid, midrecv, finrecv, rsend, rrecv, nsem, xsem):
+    sp = lax.axis_index("sp")
+    t = lax.axis_index("tp")
+    core = lax.rem(sp, 2)
+    chip = lax.div(sp, 2)
+    x = lax.rem(chip, NX)
+    z = lax.div(chip, NX)
+    t_up, t_dn, t_far = lax.rem(t + 1, 4), lax.rem(t + 3, 4), lax.rem(t + 2, 4)
+
+    def chip_at(dz, dx):
+        return lax.rem(z + dz, NZ) * NX + lax.rem(x + dx, NX)
+
+    def plane(which):
+        return {"sp": which * 2 + core}
+
+    partner = {"sp": chip * 2 + 1 - core}
+    up, dn = {"tp": t_up}, {"tp": t_dn}
+
+    loads = [
+        pltpu.make_async_copy(wg_hbm, wg, wsem.at[0]),
+        pltpu.make_async_copy(wu_hbm, wu, wsem.at[1]),
+        pltpu.make_async_copy(wd_hbm, wd, wsem.at[2]),
+    ]
+    for load in loads:
+        load.start()
+    both[core] = normed_ref[...]
+
+    barrier = pltpu.get_barrier_semaphore()
+    for peer in (partner, up, dn):
+        pl.semaphore_signal(barrier, inc=1, device_id=peer, device_id_type=MESH)
+    others = [(dz, dx) for dz in GROUP_ORDER for dx in (0, 1, 3, 2) if (dz, dx) != (0, 0)]
+    for dz, dx in others:
+        pl.semaphore_signal(barrier, inc=1, device_id=plane(chip_at(dz, dx)), device_id_type=MESH)
+    pl.semaphore_wait(barrier, 3 + len(others))
+
+    def remote(src, dst, send_sem, recv_sem, to):
+        return pltpu.make_async_remote_copy(
+            src_ref=src, dst_ref=dst, send_sem=send_sem, recv_sem=recv_sem, device_id=to, device_id_type=MESH
+        )
+
+    swap = remote(normed_ref, both.at[core], nsem.at[0], nsem.at[1], partner)
+    swap.start()
+    swap.wait()
+    tokens = jnp.concatenate([both[0], both[1]], axis=0)
+    for cut in range(4):
+        cols = slice(cut * 512, cut * 512 + 512)
+        msgs[:, :, cols] = (
+            jnp.dot(disp_ref[...], tokens[:, cols], preferred_element_type=jnp.float32)
+            .astype(jnp.bfloat16)
+            .reshape(32, 8, 512)
+        )
+
+    for dz, dx in others:
+        to = chip_at(dz, dx)
+        remote(msgs.at[to], rows.at[t, chip], msend.at[to], mrecv.at[chip], plane(to)).start()
+    rows[t, chip] = msgs[chip]
+
+    def chunk_at(which, dz):
+        first = lax.rem(z + NZ - dz, NZ) * NX
+        return rows.at[which, pl.ds(first, NX)]
+
+    def give(dz, sem, to):
+        ref = chunk_at(t, dz)
+        return remote(ref, ref, sem, grecv.at[t * 8 + dz], to)
+
+    def take(which, dz):
+        ref = chunk_at(which, dz)
+        remote(ref, ref, gup.at[0], grecv.at[which * 8 + dz], up).wait_recv()
+
+    def hand(which, dz, to):
+        ref = chunk_at(which, dz)
+        return remote(ref, ref, gfw.at[dz], grecv.at[which * 8 + dz], to)
+
+    def relay(dz):
+        take(t_dn, dz)
+        if dz in VIA_UP:
+            hand(t_dn, dz, up).start()
+        take(t_up, dz)
+        if dz in VIA_DN:
+            hand(t_up, dz, dn).start()
+
+    for i, dz in enumerate(GROUP_ORDER):
+        for dx in (0, 1, 3, 2):
+            if (dz, dx) != (0, 0):
+                source = chip_at(NZ - dz, dx)
+                remote(msgs.at[0], rows.at[t, source], msend.at[0], mrecv.at[source], partner).wait_recv()
+        give(dz, gup.at[dz], up).start()
+        give(dz, gdn.at[dz], dn).start()
+        if i > 0:
+            relay(GROUP_ORDER[i - 1])
+    for load in loads:
+        load.wait()
+
+    def serve(which):
+        data = rows[which].reshape(256, 2048)
+        for f in range(2):
+            cols = slice(f * 256, f * 256 + 256)
+            gate = jnp.minimum(jnp.dot(data, wg[:, cols], preferred_element_type=jnp.float32), clamp_limit)
+            lift = jnp.clip(jnp.dot(data, wu[:, cols], preferred_element_type=jnp.float32), -clamp_limit, clamp_limit)
+            act[:, cols] = (gate * jax.nn.sigmoid(swish_alpha * gate) * (lift + 1.0)).astype(jnp.bfloat16)
+        for cut in range(8):
+            cols = slice(cut * 256, cut * 256 + 256)
+            part[which, :, :, cols] = (
+                jnp.dot(act[...], wd[:, cols], preferred_element_type=jnp.float32).astype(jnp.bfloat16).reshape(32, 8, 256)
+            )
+
+    def group(dz):
+        return pl.ds(lax.rem(z + NZ - dz, NZ) * NX, NX)
+
+    serve(t)
+    relay(GROUP_ORDER[-1])
+    serve(t_up)
+    for k, dz in enumerate(VIA_DN):
+        remote(part.at[t_up, group(dz)], fin.at[0, group(dz)], s_direct.at[k], finrecv.at[dz], up).start()
+    serve(t_dn)
+    for k, dz in enumerate(VIA_UP):
+        remote(part.at[t_dn, group(dz)], fin.at[1, group(dz)], s_direct.at[4 + k], finrecv.at[8 + dz], dn).start()
+    for dz in GROUP_ORDER:
+        take(t_far, dz)
+    serve(t_far)
+    for k in range(4):
+        remote(part.at[t_far, group(VIA_UP[k])], mid.at[0, k], s_first.at[k], midrecv.at[k], up).start()
+        remote(part.at[t_far, group(VIA_DN[k])], mid.at[1, k], s_first.at[4 + k], midrecv.at[4 + k], dn).start()
+    for k in range(4):
+        for way, (dzs, owner, to) in enumerate(((VIA_UP, t_up, up), (VIA_DN, t_dn, dn))):
+            where = group(dzs[k])
+            remote(part.at[owner, where], mid.at[way, k], s_first.at[0], midrecv.at[way * 4 + k], up).wait_recv()
+            total = part[owner, where].astype(jnp.float32) + mid[way, k].astype(jnp.float32)
+            part[owner, where] = total.astype(jnp.bfloat16)
+            remote(part.at[owner, where], fin.at[way, where], s_mid.at[way * 4 + k], finrecv.at[way * 8 + dzs[k]], to).start()
+    for k in range(4):
+        for dz in (VIA_UP[k], VIA_DN[k]):
+            where = group(dz)
+            for way in range(2):
+                remote(part.at[t, where], fin.at[way, where], s_first.at[0], finrecv.at[way * 8 + dz], up).wait_recv()
+            total = part[t, where].astype(jnp.float32) + fin[0, where].astype(jnp.float32) + fin[1, where].astype(jnp.float32)
+            part[t, where] = total.astype(jnp.bfloat16)
+            for dx in (2, 1, 3, 0):
+                to = chip_at(NZ - dz, dx)
+                if (dz, dx) != (0, 0):
+                    remote(part.at[t, to], ret.at[chip], rsend.at[to], rrecv.at[chip], plane(to)).start()
+    ret[chip] = part[t, chip]
+    for dz, dx in others:
+        source = chip_at(dz, dx)
+        remote(part.at[t, 0], ret.at[source], rsend.at[0], rrecv.at[source], partner).wait_recv()
+    weight = mixw_ref[...]
+    coarse = weight.astype(jnp.bfloat16)
+    fine = (weight - coarse.astype(jnp.float32)).astype(jnp.bfloat16)
+    for cut in range(4):
+        cols = slice(cut * 512, cut * 512 + 512)
+        came = ret[:, :, cols].reshape(256, 512)
+        mixed = jnp.dot(coarse, came, preferred_element_type=jnp.float32) + jnp.dot(
+            fine, came, preferred_element_type=jnp.float32
+        )
+        mixs[0, :, cols] = mixed[:32]
+        mixs[1, :, cols] = mixed[32:]
+    swap_mix = remote(mixs.at[1 - core], mixs.at[2], xsem.at[0], xsem.at[1], partner)
+    swap_mix.start()
+
+    def sent(src, sem):
+        remote(src, src, sem, nsem.at[1], partner).wait_send()
+
+    for dz, dx in others:
+        to = chip_at(dz, dx)
+        sent(msgs.at[0], msend.at[to])
+        sent(msgs.at[0], rsend.at[to])
+    for i in range(8):
+        for sems in (gup, gdn, gfw, s_first, s_direct, s_mid):
+            sent(mid.at[0, 0], sems.at[i])
+    swap_mix.wait()
+    mixture = mixs[core] + mixs[2]
+    scale = lax.rsqrt(jnp.mean(mixture * mixture, axis=-1, keepdims=True) + norm_eps)
+    out_ref[...] = (middle_ref[...] + mixture * scale * gain_ref[...]).astype(jnp.bfloat16)
+
+
+def experts(normed, disp, mixw, middle, gain, w_gate, w_up, w_down):
+    whole, remote = pl.BlockSpec(memory_space=pltpu.VMEM), pl.BlockSpec(memory_space=pl.ANY)
+    dma = pltpu.SemaphoreType.DMA
+    return pl.pallas_call(
+        experts_kernel,
+        out_shape=jax.ShapeDtypeStruct((32, 2048), jnp.bfloat16),
+        in_specs=[whole] * 5 + [remote] * 3,
+        out_specs=whole,
+        scratch_shapes=[
+            pltpu.VMEM((2, 32, 2048), jnp.bfloat16),
+            pltpu.VMEM((32, 8, 2048), jnp.bfloat16),
+            pltpu.VMEM((4, 32, 8, 2048), jnp.bfloat16),
+            pltpu.VMEM((256, 512), jnp.bfloat16),
+            pltpu.VMEM((4, 32, 8, 2048), jnp.bfloat16),
+            pltpu.VMEM((2, 4, 4, 8, 2048), jnp.bfloat16),
+            pltpu.VMEM((2, 32, 8, 2048), jnp.bfloat16),
+            pltpu.VMEM((32, 8, 2048), jnp.bfloat16),
+            pltpu.VMEM((3, 32, 2048), jnp.float32),
+            pltpu.VMEM((2048, 512), jnp.bfloat16),
+            pltpu.VMEM((2048, 512), jnp.bfloat16),
+            pltpu.VMEM((512, 2048), jnp.bfloat16),
+            dma((3,)),
+            dma((32,)),
+            dma((32,)),
+            dma((8,)),
+            dma((8,)),
+            dma((8,)),
+            dma((32,)),
+            dma((8,)),
+            dma((8,)),
+            dma((8,)),
+            dma((8,)),
+            dma((16,)),
+            dma((32,)),
+            dma((32,)),
+            dma((2,)),
+            dma((2,)),
+        ],
+        compiler_params=pltpu.CompilerParams(collective_id=1, has_side_effects=True, vmem_limit_bytes=48 << 20),
+        cost_estimate=pl.CostEstimate(flops=6 * 1024 * 2048 * 512, bytes_accessed=8 << 20, transcendentals=1024 * 512),
+        name="experts",
+    )(normed, disp, mixw, middle, gain, w_gate, w_up, w_down)
+
+
 def on_device(
     queries,
     keys,
@@ -373,41 +587,10 @@
     )
     middle = residual.astype(jnp.float32) + scale_rows(projected, gain_mix)
     normed = scale_rows(middle, gain_pre).astype(jnp.bfloat16)
-    local_experts = w_gate.shape[0]
-    experts_all = local_experts * lax.axis_size("sp")
-    capacity = max(2, (2 * tok_part * TOP + experts_all - 1) // experts_all)
-    tables = slot_table(routes, experts_all, capacity)
-    chosen = jnp.sum(tables, axis=1)
-    outbound = jnp.einsum("tp,td->pd", chosen, normed, preferred_element_type=jnp.float32)
-    outbound = outbound.astype(jnp.bfloat16).reshape(experts_all, capacity, width)
-    arrived_rows = lax.all_gather(
-        lax.all_to_all(outbound, "sp", split_axis=0, concat_axis=0, tiled=True),
-        "tp",
-        axis=0,
-        tiled=True,
-    )
-    leading = arrived_rows.shape[0] // local_experts
-    partial_value = expert_apply(
-        arrived_rows.reshape(leading, local_experts, arrived_rows.shape[1], width),
-        w_gate,
-        w_up,
-        w_down,
-    )
-    summed = lax.psum_scatter(
-        partial_value.reshape(arrived_rows.shape).astype(jnp.bfloat16),
-        "tp",
-        scatter_dimension=0,
-        tiled=True,
-    )
-    returned = send_back(summed)
-    gathered = jnp.einsum(
-        "tkp,pd->tkd",
-        tables,
-        returned.reshape(experts_all * capacity, width),
-        preferred_element_type=jnp.float32,
-    )
-    mixture = jnp.sum(gathered * route_weights[:, :, None], axis=1)
-    return (middle + scale_rows(mixture, gain_moe)).astype(jnp.bfloat16)
+    disp, mixw = slot_tables(routes, route_weights)
+    return experts(
+        normed, disp, mixw, middle, gain_moe.reshape(1, width), w_gate[0], w_up[0], w_down[0]
+    )
 
 
 def solution(mesh):

time: 300 us -> 195 us (0.65)
  Pallas kernels: 64.5 us -> 170 us
  waiting for transfers between devices: 103 us -> 7.28 us
  blocking collectives: 73.9 us -> 0 us
  matrix products: 23 us -> 3.93 us
  between operations: 13.6 us -> 0.32 us
  local copies, waits for them, and re-layouts: 10.7 us -> 5.31 us
    pallas_call x0 -> x1, Pallas kernels: none -> 105 us  [experts(): pl.pallas_call(experts_kernel, out_shape=jax.ShapeDtypeStruct((32, 2048),...]
    all_to_all x2 -> x0, blocking collectives: 73.9 us -> none  [the longest x1 38.8 us: send_back(): lax.all_to_all(finished, 'sp', split_axis=0, concat_axis=0, tiled=True)]
    reduce_scatter x1 -> x0, waiting for transfers between devices: 50 us -> none  [on_device(): lax.psum_scatter(partial_value.reshape(arrived_rows.shape).astype(jnp.bfl...]
    all_gather x1 -> x0, waiting for transfers between devices: 45.8 us -> none  [on_device(): lax.all_gather(lax.all_to_all(outbound, 'sp', split_axis=0, concat_axis=0...]
    dot_general x4 -> x0, matrix products: 19.2 us -> none  [the longest x1 10.3 us: expert_apply(): jnp.einsum('serf,efd->serd', active, w_down, preferred_element_type=jnp.f...]
  transfers between devices with their start and end apart: 3 -> 2, of which waited for: 3 -> 2; matrix products, arithmetic and copies ran while one was open for 1% -> 1% of each run, Pallas kernels for 0% -> 0%
where the time goes in v2:
time: 195 us
  Pallas kernels  170 us (87%)
  waiting for transfers between devices  7.28 us (4%)
  local copies, waits for them, and re-layouts  5.31 us (3%)
  starting transfers between devices  4.7 us (2%)
  matrix products  3.93 us (2%)
  other arithmetic  3.22 us (2%)
    pallas_call x1, Pallas kernels, experts(): pl.pallas_call(experts_kernel, out_shape=jax.ShapeDtypeStruct((32, 2048),...  105 us
    pallas_call x1, Pallas kernels, attention(): pl.pallas_call(attention_kernel, out_shape=jax.ShapeDtypeStruct((128, 102...  64.5 us
    all_to_all x1, waiting for transfers between devices, sum_at_owner(): lax.all_to_all(pieces, axis, split_axis=0, concat_axis=0, tiled=True)  6.48 us
    all_to_all x1, starting transfers between devices, sum_at_owner(): lax.all_to_all(pieces, axis, split_axis=0, concat_axis=0, tiled=True)  4.19 us
    dot_general x1, matrix products, on_device(): jnp.dot(mixed_heads, w_out, preferred_element_type=jnp.float32)  3.93 us
  transfers between devices with their start and end apart: 2, of which 2 were waited for; matrix products, arithmetic and copies ran while one was open for 1% of the time, Pallas kernels for 0%

profile of v2, /device:TPU:1, one launch (start us, length us, event | category | flops | bytes accessed | tf_op | source)
XLA Modules:
  0.0 194.5 jit_solution(13377499254680744247)
XLA Ops:
  0.1 1.2 copy.54
  1.4 0.1 fusion.14
  1.5 0.8 fusion.1
  2.3 0.1 multiply_subtract_fusion
  2.5 0.8 copy.55
  3.3 0.1 copy.56
  3.5 0.1 fusion.4
  3.6 0.1 copy.57
  3.8 0.1 copy.58
  3.9 0.7 pad_maximum_fusion.kv_ref
  4.6 64.5 %gather_attention.1 = bf16[128,1024]{1,0:T(8,128)(2,1)} custom-call(bf16[2,512,128]{2,1,0:T(8,128)(2,1)} %bitcast.31, bf16[2,2,128,128]{3,2,1,0:T(8,128)(2,1)} %pad_maximum_fusion.kv_ref), custom_call_target="tpu_custom_call" | custom-call | flops 4294967296 | bytes 1048576 | tf_op jit(solution)/shard_map/gather_attention/pallas_call | solution.py:292
  69.1 3.9 %convolution_convert_fusion = bf16[128,2048]{1,0:T(8,128)(2,1)} fusion(bf16[128,1024]{1,0:T(8,128)(2,1)} %gather_attention.1, bf16[1024,2048]{1,0:T(8,128)(2,1)} %param.20), kind=kOutput, calls=%fused_computation | convolution fusion | flops 537133056 | bytes 4980736 | tf_op jit(solution)/shard_map/dot_general | solution.py:584
  73.1 4.2 %all-to-all-start = ((bf16[4,32,2048]{2,1,0:T(8,128)(2,1)}), bf16[4,32,2048]{2,1,0:T(8,128)(2,1)S(1)}, u32[]{:S(2)}, u32[]{:S(2)}) async-start(bf16[4,32,2048]{2,1,0:T(8,128)(2,1)} %bitcast.10), calls=%async_computation | async-start | bytes 1048576 | tf_op jit(solution)/shard_map/all_to_all | solution.py:26
  77.3 0.5 collective-permute-start
  77.8 0.8 collective-permute-done
  78.6 0.1 copy.59
  78.8 0.1 fusion.18
  78.9 0.1 eq.59
  79.0 0.2 select_reduce_fusion.1
  79.2 0.1 reshape.235
  79.3 0.1 fusion.10
  79.5 0.1 convert_reduce_fusion.1
  79.7 0.1 copy.63.disp_ref
  79.8 0.1 select_reduce_fusion.mixw_ref
  79.9 6.5 %all-to-all-done = bf16[4,32,2048]{2,1,0:T(8,128)(2,1)S(1)} async-done(((bf16[4,32,2048]{2,1,0:T(8,128)(2,1)}), bf16[4,32,2048]{2,1,0:T(8,128)(2,1)S(1)}, u32[]{:S(2)}, u32[]{:S(2)}) %all-to-all-start) | async-done | bytes 524320 | tf_op jit(solution)/shard_map/all_to_all | solution.py:26
  86.4 0.1 convert_reduce_fusion
  86.5 0.1 multiply_reduce_fusion.1
  86.6 0.2 multiply_reduce_fusion
  86.9 0.1 multiply_convert_fusion.normed_ref
  87.0 1.6 copy-done.1
  88.6 105.2 %experts.1 = bf16[32,2048]{1,0:T(8,128)(2,1)S(1)} custom-call(bf16[32,2048]{1,0:T(8,128)(2,1)S(1)} %multiply_convert_fusion.normed_ref, bf16[256,64]{1,0:T(8,128)(2,1)S(1)} %copy.63.disp_ref, f32[64,256]{1,0:T(8,128)S(1)} %select_reduce_fusion.mixw_ref, f32[32,2048]{1,0:T(8,128)S(1)} %get-tuple-element.6.middle_ref, f32[1,2048]{1,0:T(1,128)S(1)} %bitcast.27, ...), custom_call_target="tpu_custom_call" | custom-call | flops 6442450944 | bytes 8388608 | tf_op jit(solution)/shard_map/experts/pallas_call | solution.py:508
  193.9 0.7 copy.67
  (42 shorter events, 0.6 us)
Async XLA Ops:
  0.0 3.3 %copy-start.4 = (bf16[128,2,128]{2,1,0:T(2,128)(2,1)S(1)}, bf16[128,2,128]{2,1,0:T(2,128)(2,1)}, u32[]{:S(2)}) copy-start(bf16[128,2,128]{2,1,0:T(2,128)(2,1)} %param.16) | copy-start | bytes 196612
  0.0 3.5 %copy-start.10 = (f32[128]{0:T(128)S(1)}, f32[128]{0:T(128)}, u32[]{:S(2)}) copy-start(f32[128]{0:T(128)} %param.19) | copy-start | bytes 1540
  0.0 3.7 %copy-start.5 = (bf16[128,2,128]{2,1,0:T(2,128)(2,1)S(1)}, bf16[128,2,128]{2,1,0:T(2,128)(2,1)}, u32[]{:S(2)}) copy-start(bf16[128,2,128]{2,1,0:T(2,128)(2,1)} %param.17) | copy-start | bytes 196612
  69.1 8.2 %copy-start.8 = (s32[32,4]{0,1:T(4,128)S(1)}, s32[32,4]{0,1:T(4,128)}, u32[]{:S(2)}) copy-start(s32[32,4]{0,1:T(4,128)} %param.24) | copy-start | bytes 1540
  69.1 8.2 %copy-start.9 = (f32[32,4]{0,1:T(4,128)S(1)}, f32[32,4]{0,1:T(4,128)}, u32[]{:S(2)}) copy-start(f32[32,4]{0,1:T(4,128)} %param.25) | copy-start | bytes 1540
  69.1 17.5 %copy-start.3 = (bf16[32,2048]{1,0:T(8,128)(2,1)S(1)}, bf16[32,2048]{1,0:T(8,128)(2,1)}, u32[]{:S(2)}) copy-start(bf16[32,2048]{1,0:T(8,128)(2,1)} %param.21) | copy-start | bytes 393220
  69.1 17.5 %copy-start.7 = (f32[2048]{0:T(1024)S(1)}, f32[2048]{0:T(1024)}, u32[]{:S(2)}) copy-start(f32[2048]{0:T(1024)} %param.22) | copy-start | bytes 24580
  69.1 17.8 %copy-start.6 = (f32[2048]{0:T(1024)S(1)}, f32[2048]{0:T(1024)}, u32[]{:S(2)}) copy-start(f32[2048]{0:T(1024)} %param.23) | copy-start | bytes 24580
  69.1 17.9 %copy-start = (bf16[1,2048,512]{2,1,0:T(8,128)(2,1)S(1)}, bf16[1,2048,512]{2,1,0:T(8,128)(2,1)}, u32[]{:S(2)}) copy-start(bf16[1,2048,512]{2,1,0:T(8,128)(2,1)} %param.26) | copy-start | bytes 6291460
  69.1 17.9 %copy-start.2 = (f32[2048]{0:T(1024)S(1)}, f32[2048]{0:T(1024)}, u32[]{:S(2)}) copy-start(f32[2048]{0:T(1024)} %param.29) | copy-start | bytes 24580
  73.1 13.3 %all-to-all-start = ((bf16[4,32,2048]{2,1,0:T(8,128)(2,1)}), bf16[4,32,2048]{2,1,0:T(8,128)(2,1)S(1)}, u32[]{:S(2)}, u32[]{:S(2)}) async-start(bf16[4,32,2048]{2,1,0:T(8,128)(2,1)} %bitcast.10), calls=%async_computation | async-start | bytes 1048576 | tf_op jit(solution)/shard_map/all_to_all | solution.py:26
  77.3 1.3 collective-permute-start
  87.0 1.6 copy-start.1

commit v3 on v2

--- a/solution.py
+++ b/solution.py
@@ -13,18 +13,6 @@
 rope_theta = 10000.0
 clamp_limit = 7.0
 swish_alpha = 1.702
-
-
-def in_blocks(value, dim, devices):
-    lengths = value.shape
-    pieces = value.reshape(*lengths[:dim], devices, lengths[dim] // devices, *lengths[dim + 1 :])
-    return jnp.moveaxis(pieces, dim, 0)
-
-
-def sum_at_owner(value, axis, dim):
-    pieces = in_blocks(value, dim, lax.axis_size(axis))
-    arrived = lax.all_to_all(pieces, axis, split_axis=0, concat_axis=0, tiled=True)
-    return arrived.astype(jnp.float32).sum(axis=0)
 
 
 def rope_tables(positions, head_size):
@@ -88,8 +76,13 @@
 PIECE = 128
 
 
-def attention_kernel(q_ref, kv_ref, out_ref, buf, qbuf, m_ref, l_ref, acc, obuf, rsem, qsem, asem, zup, zdn, bup, bdn, bxp, bxm, bfw, dsem, osem):
+def attention_kernel(q_ref, kv_ref, wo_hbm, residual_ref, mix_ref, pre_ref, middle_ref, normed_ref,
+                     buf, qbuf, m_ref, l_ref, acc, obuf, heads, wo, pbuf, pin,
+                     rsem, qsem, asem, zup, zdn, bup, bdn, bxp, bxm, bfw, dsem, osem, psend, precv, wsem):
     sp = lax.axis_index("sp")
+    t = lax.axis_index("tp")
+    load = pltpu.make_async_copy(wo_hbm, wo, wsem)
+    load.start()
     core = lax.rem(sp, 2)
     chip = lax.div(sp, 2)
     x = lax.rem(chip, NX)
@@ -113,9 +106,10 @@
     acc[...] = jnp.zeros(acc.shape, jnp.float32)
 
     barrier = pltpu.get_barrier_semaphore()
-    for peer in (partner, z_up, z_dn, x_up, x_dn, x_far):
+    tp_peers = [lax.rem(t + d, 4) for d in (2, 1, 3)]
+    for peer in (partner, z_up, z_dn, x_up, x_dn, x_far, *({"tp": p} for p in tp_peers)):
         pl.semaphore_signal(barrier, inc=1, device_id=peer, device_id_type=MESH)
-    pl.semaphore_wait(barrier, 6)
+    pl.semaphore_wait(barrier, 9)
 
     def move(at, sem, to):
         return pltpu.make_async_remote_copy(
@@ -165,91 +159,99 @@
     send(own_b, bdn.at[0], z_dn)
     send(own_a, asem.at[0], x_up)
     send(own_a, asem.at[1], x_dn)
-    send(own_a, asem.at[2], x_far)
     send(own_a, zup.at[0], z_up)
     send(own_a, zdn.at[0], z_dn)
+    send(own_a, asem.at[2], x_far)
     send(own_b, bxp.at[0], x_up)
     send(own_b, bxm.at[0], x_dn)
-    for j in (1, 3, 2):
-        at = slot(A, z, x + j)
-        arrive(at)
-        send(at, zup.at[j], z_up)
-        send(at, zdn.at[j], z_dn)
+    ready = [own_a, own_b]
+
+    def work(least=4):
+        if len(ready) >= least:
+            group = ready[:4]
+            del ready[:4]
+            attend(group)
+
+    def lines_b(r):
+        lo, hi = slot(B, z - r, x), slot(B, z + r, x)
+        arrive(lo)
+        if r < 4:
+            send(lo, bup.at[r], z_up)
+        send(lo, bxp.at[2 * r - 1], x_up)
+        send(lo, bxm.at[2 * r - 1], x_dn)
+        ready.append(lo)
+        if r < 4:
+            arrive(hi)
+            if r < 3:
+                send(hi, bdn.at[r], z_dn)
+            send(hi, bxp.at[2 * r], x_up)
+            send(hi, bxm.at[2 * r], x_dn)
+            ready.append(hi)
+
+    def lines_a(r, j):
+        lo, hi = slot(A, z - r, x + j), slot(A, z + r, x + j)
+        arrive(lo)
+        if r < 3 or (r == 3 and j in (0, 1)):
+            send(lo, zup.at[r * 4 + j], z_up)
+        if 0 < r < 4:
+            ready.append(lo)
+            arrive(hi)
+        if r < 3 or (r == 3 and j in (2, 3)):
+            send(hi, zdn.at[r * 4 + j], z_dn)
+        ready.append(hi)
+
+    def across(r):
+        if r > 0:
+            at = slot(B, z - r, x - 1)
+            arrive(at)
+            send(at, bfw.at[2 * r - 1], x_up)
+            ready.append(at)
+        if r < 4:
+            at = slot(B, z + r, x + 1)
+            arrive(at)
+            send(at, bfw.at[2 * r], x_dn)
+            ready.append(at)
+        if r > 0:
+            at = slot(B, z - r, x + 1)
+            arrive(at)
+            ready.append(at)
+        if r < 4:
+            at = slot(B, z + r, x - 1)
+            arrive(at)
+            ready.append(at)
+
+    def far(r):
+        for at in {0: [slot(B, z, x + 2)], 4: [slot(B, z + 4, x + 2)]}.get(r, [slot(B, z - r, x + 2), slot(B, z + r, x + 2)]):
+            arrive(at)
+            ready.append(at)
+
+    lines_a(0, 1)
+    lines_a(0, 3)
+    lines_a(0, 2)
     swap_q.wait_recv()
-    attend([own_a, own_b, slot(A, z, x + 1), slot(A, z, x + 3)])
-    left, right, far = slot(B, z, x - 1), slot(B, z, x + 1), slot(B, z, x + 2)
-    arrive(right)
-    send(right, bfw.at[0], x_dn)
-    arrive(left)
-
-    def step(r, last):
-        lo, hi = z - r, z + r
-        b_lo, b_hi = slot(B, lo, x), slot(B, hi, x)
-        arrive(b_lo)
-        send(b_lo, bup.at[r], z_up)
-        send(b_lo, bxp.at[2 * r - 1], x_up)
-        send(b_lo, bxm.at[2 * r - 1], x_dn)
-        arrive(b_hi)
-
-        @pl.when(r < 3)
-        def _():
-            send(b_hi, bdn.at[r], z_dn)
-
-        send(b_hi, bxp.at[2 * r], x_up)
-        send(b_hi, bxm.at[2 * r], x_dn)
-        for pair in ((0, 1), (3, 2)):
-            group = []
-            for j in pair:
-                a_lo, a_hi = slot(A, lo, x + j), slot(A, hi, x + j)
-                group += [a_lo, a_hi]
-                arrive(a_lo)
-                if j in (0, 1):
-                    send(a_lo, zup.at[r * 4 + j], z_up)
-                else:
-                    pl.when(r < 3)(lambda a_lo=a_lo, j=j: send(a_lo, zup.at[r * 4 + j], z_up))
-                arrive(a_hi)
-                if j in (2, 3):
-                    send(a_hi, zdn.at[r * 4 + j], z_dn)
-                else:
-                    pl.when(r < 3)(lambda a_hi=a_hi, j=j: send(a_hi, zdn.at[r * 4 + j], z_dn))
-            attend(group)
-        lo_left, lo_right, lo_far = slot(B, lo, x - 1), slot(B, lo, x + 1), slot(B, lo, x + 2)
-        hi_left, hi_right, hi_far = slot(B, hi, x - 1), slot(B, hi, x + 1), slot(B, hi, x + 2)
-        arrive(lo_left)
-        send(lo_left, bfw.at[2 * r - 1], x_up)
-        arrive(hi_right)
-        send(hi_right, bfw.at[2 * r], x_dn)
-        attend([b_lo, b_hi, lo_left, hi_right])
-        arrive(lo_right)
-        arrive(hi_left)
-        arrive(lo_far)
-        arrive(hi_far)
-        attend([lo_right, hi_left, lo_far, hi_far])
-
-    arrive(far)
-    attend([slot(A, z, x + 2), left, right, far])
-
-    @pl.loop(1, 4)
-    def _(r):
-        step(r, False)
-
-    opp = z + 4
-    b_op = slot(B, opp, x)
-    arrive(b_op)
-    send(b_op, bxp.at[7], x_up)
-    send(b_op, bxm.at[7], x_dn)
-    group = []
-    for j in (0, 1, 3, 2):
-        at = slot(A, opp, x + j)
-        arrive(at)
-        group.append(at)
-    b_left, b_right, b_far = slot(B, opp, x - 1), slot(B, opp, x + 1), slot(B, opp, x + 2)
-    arrive(b_left)
-    send(b_left, bfw.at[7], x_up)
-    attend(group)
-    arrive(b_right)
-    arrive(b_far)
-    attend([b_op, b_left, b_right, b_far])
+    for r in range(1, 5):
+        lines_b(r)
+        work()
+        lines_a(r, 0)
+        work()
+        lines_a(r, 1)
+        work()
+        across(r - 1)
+        work()
+        lines_a(r, 3)
+        work()
+        lines_a(r, 2)
+        work()
+        if r > 1:
+            far(r - 2)
+        work()
+    across(4)
+    work()
+    far(3)
+    work()
+    far(4)
+    while ready:
+        work(1)
 
     def heads_of(which):
         cols = pl.ds(pl.multiple_of(which * 512, 512), 512)
@@ -263,6 +265,30 @@
         src_ref=obuf.at[2], dst_ref=obuf.at[core], send_sem=osem.at[0], recv_sem=osem.at[1], device_id=partner, device_id_type=MESH
     )
     swap_o.start()
+
+    def stack_heads(g):
+        for h in range(4):
+            cols = pl.ds(pl.multiple_of(g * 512 + h * 128, 128), 128)
+            heads[:, cols] = obuf[g, :, h * 128 : h * 128 + 128].T
+
+    stack_heads(core)
+    load.wait()
+    swap_o.wait()
+    stack_heads(1 - core)
+    for cut in range(4):
+        cols = slice(cut * 512, cut * 512 + 512)
+        part = jnp.dot(heads[...], wo[:, cols], preferred_element_type=jnp.float32).astype(jnp.bfloat16)
+        for owner in range(4):
+            pbuf[owner, :, cols] = part[owner * 32 : owner * 32 + 32]
+    gives = [
+        pltpu.make_async_remote_copy(
+            src_ref=pbuf.at[peer], dst_ref=pin.at[i], send_sem=psend.at[i], recv_sem=precv.at[i], device_id={"tp": peer},
+            device_id_type=MESH,
+        )
+        for i, peer in enumerate(tp_peers)
+    ]
+    for give in gives:
+        give.start()
     for i in range(3):
         done(asem.at[i])
     for i in range(4):
@@ -280,20 +306,23 @@
         done(bfw.at[i])
     swap_kv.wait_send()
     swap_q.wait_send()
-    swap_o.wait_send()
-    swap_o.wait_recv()
-    for g in range(2):
-        for h in range(4):
-            head = obuf[g, :, h * 128 : h * 128 + 128]
-            out_ref[:, (g * 4 + h) * 128 : (g * 4 + h) * 128 + 128] = head.T
-
-
-def attention(q_two, kv_two):
+    for give in gives:
+        give.wait()
+    projected = pbuf[t].astype(jnp.float32)
+    for i in range(3):
+        projected = projected + pin[i].astype(jnp.float32)
+    middle = residual_ref[...].astype(jnp.float32) + scale_rows(projected, mix_ref[...])
+    middle_ref[...] = middle
+    normed_ref[...] = scale_rows(middle, pre_ref[...]).astype(jnp.bfloat16)
+
+
+def attention(q_two, kv_two, w_out, residual, gain_mix, gain_pre):
+    whole, apart = pl.BlockSpec(memory_space=pltpu.VMEM), pl.BlockSpec(memory_space=pl.ANY)
     return pl.pallas_call(
         attention_kernel,
-        out_shape=jax.ShapeDtypeStruct((128, 1024), jnp.bfloat16),
-        in_specs=[pl.BlockSpec(memory_space=pltpu.VMEM)] * 2,
-        out_specs=pl.BlockSpec(memory_space=pltpu.VMEM),
+        out_shape=[jax.ShapeDtypeStruct((32, 2048), jnp.float32), jax.ShapeDtypeStruct((32, 2048), jnp.bfloat16)],
+        in_specs=[whole, whole, apart, whole, whole, whole],
+        out_specs=[whole, whole],
         scratch_shapes=[
             pltpu.VMEM((64, 2, PIECE, 128), jnp.bfloat16),
             pltpu.VMEM((1024, 128), jnp.bfloat16),
@@ -301,6 +330,10 @@
             pltpu.VMEM((1, 1024), jnp.float32),
             pltpu.VMEM((128, 1024), jnp.float32),
             pltpu.VMEM((3, 128, 512), jnp.bfloat16),
+            pltpu.VMEM((128, 1024), jnp.bfloat16),
+            pltpu.VMEM((1024, 2048), jnp.bfloat16),
+            pltpu.VMEM((4, 32, 2048), jnp.bfloat16),
+            pltpu.VMEM((3, 32, 2048), jnp.bfloat16),
             pltpu.SemaphoreType.DMA((64,)),
             pltpu.SemaphoreType.DMA,
             pltpu.SemaphoreType.DMA((3,)),
@@ -313,11 +346,14 @@
             pltpu.SemaphoreType.DMA((8,)),
             pltpu.SemaphoreType.DMA((2,)),
             pltpu.SemaphoreType.DMA((2,)),
+            pltpu.SemaphoreType.DMA((3,)),
+            pltpu.SemaphoreType.DMA((3,)),
+            pltpu.SemaphoreType.DMA,
         ],
-        compiler_params=pltpu.CompilerParams(collective_id=0, has_side_effects=True),
+        compiler_params=pltpu.CompilerParams(collective_id=0, has_side_effects=True, vmem_limit_bytes=40 << 20),
         cost_estimate=pl.CostEstimate(flops=4 * 1024 * 8192 * 128, bytes_accessed=1 << 20, transcendentals=1024 * 8192),
         name="gather_attention",
-    )(q_two, kv_two)
+    )(q_two, kv_two, w_out, residual, gain_mix, gain_pre)
 
 
 GROUP_ORDER = (0, 1, 7, 2, 6, 3, 5, 4)
@@ -438,26 +474,26 @@
 
     serve(t)
     relay(GROUP_ORDER[-1])
-    serve(t_up)
-    for k, dz in enumerate(VIA_DN):
-        remote(part.at[t_up, group(dz)], fin.at[0, group(dz)], s_direct.at[k], finrecv.at[dz], up).start()
-    serve(t_dn)
-    for k, dz in enumerate(VIA_UP):
-        remote(part.at[t_dn, group(dz)], fin.at[1, group(dz)], s_direct.at[4 + k], finrecv.at[8 + dz], dn).start()
-    for dz in GROUP_ORDER:
-        take(t_far, dz)
-    serve(t_far)
-    for k in range(4):
-        remote(part.at[t_far, group(VIA_UP[k])], mid.at[0, k], s_first.at[k], midrecv.at[k], up).start()
-        remote(part.at[t_far, group(VIA_DN[k])], mid.at[1, k], s_first.at[4 + k], midrecv.at[4 + k], dn).start()
-    for k in range(4):
+
+    def direct(k):
+        a, b = group(VIA_DN[k]), group(VIA_UP[k])
+        remote(part.at[t_up, a], fin.at[0, a], s_direct.at[k], finrecv.at[VIA_DN[k]], up).start()
+        remote(part.at[t_dn, b], fin.at[1, b], s_direct.at[4 + k], finrecv.at[8 + VIA_UP[k]], dn).start()
+
+    def first(k):
+        a, b = group(VIA_UP[k]), group(VIA_DN[k])
+        remote(part.at[t_far, a], mid.at[0, k], s_first.at[k], midrecv.at[k], up).start()
+        remote(part.at[t_far, b], mid.at[1, k], s_first.at[4 + k], midrecv.at[4 + k], dn).start()
+
+    def middle_sum(k):
         for way, (dzs, owner, to) in enumerate(((VIA_UP, t_up, up), (VIA_DN, t_dn, dn))):
             where = group(dzs[k])
             remote(part.at[owner, where], mid.at[way, k], s_first.at[0], midrecv.at[way * 4 + k], up).wait_recv()
             total = part[owner, where].astype(jnp.float32) + mid[way, k].astype(jnp.float32)
             part[owner, where] = total.astype(jnp.bfloat16)
             remote(part.at[owner, where], fin.at[way, where], s_mid.at[way * 4 + k], finrecv.at[way * 8 + dzs[k]], to).start()
-    for k in range(4):
+
+    def settle(k):
         for dz in (VIA_UP[k], VIA_DN[k]):
             where = group(dz)
             for way in range(2):
@@ -468,6 +504,28 @@
                 to = chip_at(NZ - dz, dx)
                 if (dz, dx) != (0, 0):
                     remote(part.at[t, to], ret.at[chip], rsend.at[to], rrecv.at[chip], plane(to)).start()
+
+    serve(t_up)
+    serve(t_dn)
+    direct(0)
+    for dz in GROUP_ORDER:
+        take(t_far, dz)
+    serve(t_far)
+    first(0)
+    first(1)
+    middle_sum(0)
+    direct(1)
+    first(2)
+    middle_sum(1)
+    settle(0)
+    direct(2)
+    first(3)
+    middle_sum(2)
+    settle(1)
+    direct(3)
+    middle_sum(3)
+    settle(2)
+    settle(3)
     ret[chip] = part[t, chip]
     for dz, dx in others:
         source = chip_at(dz, dx)
@@ -577,16 +635,10 @@
     )
     q_two = q_turned.transpose(1, 0, 2).reshape(kv_local, group_size * tok_rows, head_size)
     kv_two = jnp.stack([k_turned.transpose(1, 0, 2), values.transpose(1, 2, 0)], axis=1)
-    mixed_heads = attention(q_two, kv_two)
-    tok_part = residual.shape[0]
     width = residual.shape[1]
-    projected = sum_at_owner(
-        jnp.dot(mixed_heads, w_out, preferred_element_type=jnp.float32).astype(jnp.bfloat16),
-        "tp",
-        0,
-    )
-    middle = residual.astype(jnp.float32) + scale_rows(projected, gain_mix)
-    normed = scale_rows(middle, gain_pre).astype(jnp.bfloat16)
+    middle, normed = attention(
+        q_two, kv_two, w_out, residual, gain_mix.reshape(1, width), gain_pre.reshape(1, width)
+    )
     disp, mixw = slot_tables(routes, route_weights)
     return experts(
         normed, disp, mixw, middle, gain_moe.reshape(1, width), w_gate[0], w_up[0], w_down[0]

time: 195 us -> 169 us (0.87)
  Pallas kernels: 170 us -> 155 us
  waiting for transfers between devices: 7.28 us -> 0.01 us
  matrix products: 3.93 us -> 0 us
    pallas_call x1, Pallas kernels: 105 us -> 96.6 us  [experts(): pl.pallas_call(experts_kernel, out_shape=jax.ShapeDtypeStruct((32, 2048),...]
    pallas_call x1, Pallas kernels: 64.5 us -> 58 us  [attention(): pl.pallas_call(attention_kernel, out_shape=[jax.ShapeDtypeStruct((32, 204...]
    all_to_all x1 -> x0, waiting for transfers between devices: 6.48 us -> none  [sum_at_owner(): lax.all_to_all(pieces, axis, split_axis=0, concat_axis=0, tiled=True)]
    all_to_all x1 -> x0, starting transfers between devices: 4.19 us -> none  [sum_at_owner(): lax.all_to_all(pieces, axis, split_axis=0, concat_axis=0, tiled=True)]
    dot_general x1 -> x0, matrix products: 3.93 us -> none  [on_device(): jnp.dot(mixed_heads, w_out, preferred_element_type=jnp.float32)]
    ppermute x1, starting transfers between devices: 0.52 us -> 3.2 us  [slot_tables(): other = lax.ppermute(both, 'sp', swap)]
    unnamed x26 -> x24, local copies, waits for them, and re-layouts: 3.72 us -> 5.87 us
  transfers between devices with their start and end apart: 2 -> 1, of which waited for: 2 -> 0; matrix products, arithmetic and copies ran while one was open for 1% -> 2% of each run, Pallas kernels for 0% -> 34%
where the time goes in v3:
time: 169 us; the launch traced here: 168 us
  Pallas kernels  155 us (92%)
  local copies, waits for them, and re-layouts  6.79 us (4%)
  other arithmetic  3.44 us (2%)
  starting transfers between devices  3.2 us (2%)
    pallas_call x1, Pallas kernels, experts(): pl.pallas_call(experts_kernel, out_shape=jax.ShapeDtypeStruct((32, 2048),...  96.6 us
    pallas_call x1, Pallas kernels, attention(): pl.pallas_call(attention_kernel, out_shape=[jax.ShapeDtypeStruct((32, 204...  58 us
    unnamed x24, local copies, waits for them, and re-layouts  5.87 us
  transfers between devices with their start and end apart: 1, of which 0 were waited for; matrix products, arithmetic and copies ran while one was open for 2% of the time, Pallas kernels for 34%

profile of v3, /device:TPU:1, one launch (start us, length us, event | category | flops | bytes accessed | tf_op | source)
XLA Modules:
  0.0 168.4 jit_solution(6943530278140869232)
XLA Ops:
  0.0 0.7 convert_element_type.57
  0.7 0.7 fusion.17
  1.4 3.2 %collective-permute-start = (f32[32,8]{0,1:T(8,128)S(1)}, f32[32,8]{0,1:T(8,128)S(1)}, u32[]{:S(2)}, u32[]{:S(2)}) collective-permute-start(f32[32,8]{0,1:T(8,128)S(1)} %get-tuple-element.20), channel_id=1, source_target_pairs={{0,4},{4,0},{8,12},{12,8},{16,20},{20,16},{24,28},{28,24},{32,36},... | collective-permute-start | bytes 3080 | tf_op jit(solution)/shard_map/ppermute | solution.py:57
  4.6 1.2 copy.54
  5.8 0.1 fusion
  5.9 0.1 broadcast_multiply_fusion.1
  6.0 0.1 fusion.14
  6.1 0.8 fusion.1
  7.0 0.1 multiply_subtract_fusion
  7.1 0.1 fusion.2
  7.1 0.2 copy.55
  7.3 0.1 copy.56
  7.5 0.1 fusion.4
  7.7 0.1 copy.57
  7.8 0.1 copy.58
  8.0 2.2 %copy-done = bf16[1024,2048]{1,0:T(8,128)(2,1)S(1)} copy-done((bf16[1024,2048]{1,0:T(8,128)(2,1)S(1)}, bf16[1024,2048]{1,0:T(8,128)(2,1)}, u32[]{:S(2)}) %copy-start) | copy-done | bytes 4194328
  10.2 58.0 %gather_attention.1 = (f32[32,2048]{1,0:T(8,128)S(1)}, bf16[32,2048]{1,0:T(8,128)(2,1)S(1)}) custom-call(bf16[2,512,128]{2,1,0:T(8,128)(2,1)S(1)} %bitcast.24, bf16[2,2,128,128]{3,2,1,0:T(8,128)(2,1)S(1)} %pad_maximum_fusion.kv_ref, bf16[1024,2048]{1,0:T(8,128)(2,1)S(1)} %copy-done, bf16[32,2048]{1,0:T(8,128)(2,1)S(1)} %copy-done.3, f32[1,2048]{1,0:T(1,128)S(1)} %bitcast.27, ...), custom_call_target="tpu_custom_call" | custom-call | flops 4294967296 | bytes 1048576 | tf_op jit(solution)/shard_map/gather_attention/pallas_call | solution.py:321
  68.2 0.1 copy.59
  68.3 0.1 copy.60
  68.4 0.1 fusion.18
  68.5 0.1 eq.59
  68.6 0.2 select_reduce_fusion.1
  68.7 0.1 reshape.221
  68.9 0.1 fusion.10
  68.9 0.1 copy.64
  69.0 0.1 copy.65
  69.1 0.1 convert_reduce_fusion
  69.2 0.1 select_reduce_fusion.mixw_ref
  69.4 0.1 copy.63.disp_ref
  69.5 1.6 copy-done.2
  71.1 96.6 %experts.1 = bf16[32,2048]{1,0:T(8,128)(2,1)S(1)} custom-call(bf16[32,2048]{1,0:T(8,128)(2,1)S(1)} %get-tuple-element.7.normed_ref, bf16[256,64]{1,0:T(8,128)(2,1)S(1)} %copy.63.disp_ref, f32[64,256]{1,0:T(8,128)S(1)} %select_reduce_fusion.mixw_ref, f32[32,2048]{1,0:T(8,128)S(1)} %get-tuple-element.8.middle_ref, f32[1,2048]{1,0:T(1,128)S(1)} %bitcast.29, ...), custom_call_target="tpu_custom_call" | custom-call | flops 6442450944 | bytes 8388608 | tf_op jit(solution)/shard_map/experts/pallas_call | solution.py:566
  167.7 0.7 copy.67
  (31 shorter events, 0.2 us)
Async XLA Ops:
  1.4 66.8 %collective-permute-start = (f32[32,8]{0,1:T(8,128)S(1)}, f32[32,8]{0,1:T(8,128)S(1)}, u32[]{:S(2)}, u32[]{:S(2)}) collective-permute-start(f32[32,8]{0,1:T(8,128)S(1)} %get-tuple-element.20), channel_id=1, source_target_pairs={{0,4},{4,0},{8,12},{12,8},{16,20},{20,16},{24,28},{28,24},{32,36},... | collective-permute-start | bytes 3080 | tf_op jit(solution)/shard_map/ppermute | solution.py:57
  4.6 2.7 %copy-start.7 = (bf16[128,2,128]{2,1,0:T(2,128)(2,1)S(1)}, bf16[128,2,128]{2,1,0:T(2,128)(2,1)}, u32[]{:S(2)}) copy-start(bf16[128,2,128]{2,1,0:T(2,128)(2,1)} %param.16) | copy-start | bytes 196612
  4.6 2.9 %copy-start.9 = (f32[128]{0:T(128)S(1)}, f32[128]{0:T(128)}, u32[]{:S(2)}) copy-start(f32[128]{0:T(128)} %param.19) | copy-start | bytes 1540
  6.1 1.7 %copy-start.8 = (bf16[128,2,128]{2,1,0:T(2,128)(2,1)S(1)}, bf16[128,2,128]{2,1,0:T(2,128)(2,1)}, u32[]{:S(2)}) copy-start(bf16[128,2,128]{2,1,0:T(2,128)(2,1)} %param.17) | copy-start | bytes 196612
  6.1 1.8 %copy-start.3 = (bf16[32,2048]{1,0:T(8,128)(2,1)S(1)}, bf16[32,2048]{1,0:T(8,128)(2,1)}, u32[]{:S(2)}) copy-start(bf16[32,2048]{1,0:T(8,128)(2,1)} %residual_ref.1) | copy-start | bytes 393220
  6.1 1.8 %copy-start.4 = (f32[2048]{0:T(1024)S(1)}, f32[2048]{0:T(1024)}, u32[]{:S(2)}) copy-start(f32[2048]{0:T(1024)} %param.22) | copy-start | bytes 24580
  6.1 1.8 %copy-start.5 = (f32[2048]{0:T(1024)S(1)}, f32[2048]{0:T(1024)}, u32[]{:S(2)}) copy-start(f32[2048]{0:T(1024)} %param.23) | copy-start | bytes 24580
  8.0 2.2 %copy-start = (bf16[1024,2048]{1,0:T(8,128)(2,1)S(1)}, bf16[1024,2048]{1,0:T(8,128)(2,1)}, u32[]{:S(2)}) copy-start(bf16[1024,2048]{1,0:T(8,128)(2,1)} %wo_hbm.1) | copy-start | bytes 12582916
  10.2 59.3 %copy-start.1 = (bf16[1,2048,512]{2,1,0:T(8,128)(2,1)S(1)}, bf16[1,2048,512]{2,1,0:T(8,128)(2,1)}, u32[]{:S(2)}) copy-start(bf16[1,2048,512]{2,1,0:T(8,128)(2,1)} %param.26) | copy-start | bytes 6291460
  10.2 59.3 %copy-start.6 = (f32[2048]{0:T(1024)S(1)}, f32[2048]{0:T(1024)}, u32[]{:S(2)}) copy-start(f32[2048]{0:T(1024)} %param.29) | copy-start | bytes 24580
  69.5 1.6 copy-start.2

commit v4 on v3

--- a/solution.py
+++ b/solution.py
@@ -49,26 +49,17 @@
     )
 
 
-def slot_tables(routes, route_weights):
+def route_info(routes, route_weights):
     core = lax.rem(lax.axis_index("sp"), 2)
-    swap = [(i, i ^ 1) for i in range(lax.axis_size("sp"))]
     count = routes.shape[0]
-    both = jnp.concatenate([routes.astype(jnp.float32), route_weights], axis=1)
-    other = lax.ppermute(both, "sp", swap)
-    ordered = jnp.where(core == 0, jnp.stack([both, other]), jnp.stack([other, both]))
-    chosen, weights = ordered[:, :, :TOP].astype(jnp.int32), ordered[:, :, TOP:]
-    flat = chosen.reshape(2, count * TOP)
-    same = (flat[:, :, None] == flat[:, None, :]).astype(jnp.int32)
+    flat = routes.reshape(-1)
     place = jnp.arange(count * TOP, dtype=jnp.int32)
-    earlier = (place[None, :] < place[:, None]).astype(jnp.int32)
-    rank = jnp.sum(same * earlier, axis=2).reshape(2, count, TOP)
-    side = jnp.arange(2, dtype=jnp.int32)[:, None, None]
-    target = jnp.where(chosen % 2 == core, (chosen // 2) * 8 + side * 4 + rank, -1)
-    target, weights = target.reshape(2 * count, TOP), weights.reshape(2 * count, TOP)
-    spots = jnp.arange(256, dtype=jnp.int32)
-    disp = jnp.sum((target[None, :, :] == spots[:, None, None]).astype(jnp.float32), axis=2)
-    mixw = jnp.sum(jnp.where(target[:, None, :] == spots[None, :, None], weights[:, None, :], 0.0), axis=2)
-    return disp.astype(jnp.bfloat16), mixw
+    earlier = (flat[:, None] == flat[None, :]) & (place[None, :] < place[:, None])
+    rank = jnp.sum(earlier.astype(jnp.int32), axis=1)
+    slots = (flat * 4 + rank).reshape(count, TOP).astype(jnp.float32)
+    info = jnp.concatenate([slots.T, route_weights.T], axis=0)
+    side = jnp.arange(128 // count, dtype=jnp.int32)[None, :, None]
+    return jnp.where(side == core, info[:, None, :], 0.0).reshape(2 * TOP, 128)
 
 
 MESH = pl.DeviceIdType.MESH
@@ -76,7 +67,7 @@
 PIECE = 128
 
 
-def attention_kernel(q_ref, kv_ref, wo_hbm, residual_ref, mix_ref, pre_ref, middle_ref, normed_ref,
+def attention_part(q_ref, kv_ref, wo_hbm, residual_ref, mix_ref, pre_ref, middle_ref, normed_ref, meet,
                      buf, qbuf, m_ref, l_ref, acc, obuf, heads, wo, pbuf, pin,
                      rsem, qsem, asem, zup, zdn, bup, bdn, bxp, bxm, bfw, dsem, osem, psend, precv, wsem):
     sp = lax.axis_index("sp")
@@ -105,11 +96,8 @@
     l_ref[...] = jnp.zeros(l_ref.shape, jnp.float32)
     acc[...] = jnp.zeros(acc.shape, jnp.float32)
 
-    barrier = pltpu.get_barrier_semaphore()
     tp_peers = [lax.rem(t + d, 4) for d in (2, 1, 3)]
-    for peer in (partner, z_up, z_dn, x_up, x_dn, x_far, *({"tp": p} for p in tp_peers)):
-        pl.semaphore_signal(barrier, inc=1, device_id=peer, device_id_type=MESH)
-    pl.semaphore_wait(barrier, 9)
+    meet()
 
     def move(at, sem, to):
         return pltpu.make_async_remote_copy(
@@ -316,54 +304,15 @@
     normed_ref[...] = scale_rows(middle, pre_ref[...]).astype(jnp.bfloat16)
 
 
-def attention(q_two, kv_two, w_out, residual, gain_mix, gain_pre):
-    whole, apart = pl.BlockSpec(memory_space=pltpu.VMEM), pl.BlockSpec(memory_space=pl.ANY)
-    return pl.pallas_call(
-        attention_kernel,
-        out_shape=[jax.ShapeDtypeStruct((32, 2048), jnp.float32), jax.ShapeDtypeStruct((32, 2048), jnp.bfloat16)],
-        in_specs=[whole, whole, apart, whole, whole, whole],
-        out_specs=[whole, whole],
-        scratch_shapes=[
-            pltpu.VMEM((64, 2, PIECE, 128), jnp.bfloat16),
-            pltpu.VMEM((1024, 128), jnp.bfloat16),
-            pltpu.VMEM((1, 1024), jnp.float32),
-            pltpu.VMEM((1, 1024), jnp.float32),
-            pltpu.VMEM((128, 1024), jnp.float32),
-            pltpu.VMEM((3, 128, 512), jnp.bfloat16),
-            pltpu.VMEM((128, 1024), jnp.bfloat16),
-            pltpu.VMEM((1024, 2048), jnp.bfloat16),
-            pltpu.VMEM((4, 32, 2048), jnp.bfloat16),
-            pltpu.VMEM((3, 32, 2048), jnp.bfloat16),
-            pltpu.SemaphoreType.DMA((64,)),
-            pltpu.SemaphoreType.DMA,
-            pltpu.SemaphoreType.DMA((3,)),
-            pltpu.SemaphoreType.DMA((16,)),
-            pltpu.SemaphoreType.DMA((16,)),
-            pltpu.SemaphoreType.DMA((4,)),
-            pltpu.SemaphoreType.DMA((4,)),
-            pltpu.SemaphoreType.DMA((8,)),
-            pltpu.SemaphoreType.DMA((8,)),
-            pltpu.SemaphoreType.DMA((8,)),
-            pltpu.SemaphoreType.DMA((2,)),
-            pltpu.SemaphoreType.DMA((2,)),
-            pltpu.SemaphoreType.DMA((3,)),
-            pltpu.SemaphoreType.DMA((3,)),
-            pltpu.SemaphoreType.DMA,
-        ],
-        compiler_params=pltpu.CompilerParams(collective_id=0, has_side_effects=True, vmem_limit_bytes=40 << 20),
-        cost_estimate=pl.CostEstimate(flops=4 * 1024 * 8192 * 128, bytes_accessed=1 << 20, transcendentals=1024 * 8192),
-        name="gather_attention",
-    )(q_two, kv_two, w_out, residual, gain_mix, gain_pre)
-
-
 GROUP_ORDER = (0, 1, 7, 2, 6, 3, 5, 4)
 VIA_UP = (3, 6, 1, 0)
 VIA_DN = (4, 5, 2, 7)
 
 
-def experts_kernel(normed_ref, disp_ref, mixw_ref, middle_ref, gain_ref, wg_hbm, wu_hbm, wd_hbm, out_ref,
-                   both, msgs, rows, act, part, mid, fin, ret, mixs, wg, wu, wd,
-                   wsem, msend, mrecv, gup, gdn, gfw, grecv, s_first, s_direct, s_mid, midrecv, finrecv, rsend, rrecv, nsem, xsem):
+def experts_part(normed_ref, info_ref, middle_ref, gain_ref, loads, out_ref, others, column,
+                 toks, infos, msgs, rows, act, part, mid, fin, ret, mixs, wg, wu, wd,
+                   isend, irecv, tsend, trecv, msend, mrecv, gup, gdn, gfw, grecv, s_first, s_direct, s_mid, midrecv, finrecv,
+                   rsend, rrecv, xsem):
     sp = lax.axis_index("sp")
     t = lax.axis_index("tp")
     core = lax.rem(sp, 2)
@@ -381,44 +330,67 @@
     partner = {"sp": chip * 2 + 1 - core}
     up, dn = {"tp": t_up}, {"tp": t_dn}
 
-    loads = [
-        pltpu.make_async_copy(wg_hbm, wg, wsem.at[0]),
-        pltpu.make_async_copy(wu_hbm, wu, wsem.at[1]),
-        pltpu.make_async_copy(wd_hbm, wd, wsem.at[2]),
-    ]
-    for load in loads:
-        load.start()
-    both[core] = normed_ref[...]
-
-    barrier = pltpu.get_barrier_semaphore()
-    for peer in (partner, up, dn):
-        pl.semaphore_signal(barrier, inc=1, device_id=peer, device_id_type=MESH)
-    others = [(dz, dx) for dz in GROUP_ORDER for dx in (0, 1, 3, 2) if (dz, dx) != (0, 0)]
-    for dz, dx in others:
-        pl.semaphore_signal(barrier, inc=1, device_id=plane(chip_at(dz, dx)), device_id_type=MESH)
-    pl.semaphore_wait(barrier, 3 + len(others))
+    toks[z, core] = normed_ref[...]
+    infos[z, core] = info_ref[...]
+
+    column = [{"sp": to} for to in column]
 
     def remote(src, dst, send_sem, recv_sem, to):
         return pltpu.make_async_remote_copy(
             src_ref=src, dst_ref=dst, send_sem=send_sem, recv_sem=recv_sem, device_id=to, device_id_type=MESH
         )
 
-    swap = remote(normed_ref, both.at[core], nsem.at[0], nsem.at[1], partner)
-    swap.start()
-    swap.wait()
-    tokens = jnp.concatenate([both[0], both[1]], axis=0)
-    for cut in range(4):
-        cols = slice(cut * 512, cut * 512 + 512)
-        msgs[:, :, cols] = (
-            jnp.dot(disp_ref[...], tokens[:, cols], preferred_element_type=jnp.float32)
-            .astype(jnp.bfloat16)
-            .reshape(32, 8, 512)
-        )
-
-    for dz, dx in others:
-        to = chip_at(dz, dx)
-        remote(msgs.at[to], rows.at[t, chip], msend.at[to], mrecv.at[chip], plane(to)).start()
-    rows[t, chip] = msgs[chip]
+    z_up, z_dn = plane(chip_at(1, 0)), plane(chip_at(NZ - 1, 0))
+    for i, to in enumerate((partner, z_up, z_dn)):
+        remote(normed_ref, toks.at[z, core], tsend.at[i], trecv.at[z * 2 + core], to).start()
+        if i == 0:
+            remote(info_ref, infos.at[z, core], isend.at[0], irecv.at[z * 2 + core], partner).start()
+    column += [plane(chip_at(dz, 0)) for dz in range(1, NZ)]
+    for i, to in enumerate(column):
+        remote(info_ref, infos.at[z, core], isend.at[1 + i], irecv.at[z * 2 + core], to).start()
+
+    def wanted(count, first):
+        row = lax.broadcasted_iota(jnp.int32, (count, 128), 0)
+        lane = lax.broadcasted_iota(jnp.int32, (count, 128), 1)
+        expert = (first + row // 8) * 2 + core
+        slot_id = expert * 4 + row % 4
+        return jnp.where((row // 4) % 2 == lane // 32, slot_id, -1).astype(jnp.float32)
+
+    here = wanted(32, z * NX)
+
+    def hop(dz, i, to):
+        zz = lax.rem(z + NZ - dz, NZ)
+        remote(toks.at[zz, core], toks.at[zz, core], tsend.at[i], trecv.at[zz * 2 + core], to).start()
+
+    def tokens_of(dz):
+        zz = lax.rem(z + NZ - dz, NZ)
+        if dz:
+            remote(normed_ref, toks.at[zz, core], tsend.at[0], trecv.at[zz * 2 + core], partner).wait_recv()
+            if dz in (1, 2, 3):
+                hop(dz, 2 + dz, z_up)
+            if dz in (7, 6):
+                hop(dz, dz, z_dn)
+            hop(dz, 7 + dz, partner)
+            remote(info_ref, infos.at[zz, core], isend.at[0], irecv.at[zz * 2 + core], partner).wait_recv()
+        remote(info_ref, infos.at[zz, 1 - core], isend.at[0], irecv.at[zz * 2 + 1 - core], partner).wait_recv()
+        remote(normed_ref, toks.at[zz, 1 - core], tsend.at[0], trecv.at[zz * 2 + 1 - core], partner).wait_recv()
+        info = infos[zz, 0] + infos[zz, 1]
+        disp = jnp.zeros((32, 128), jnp.float32)
+        for k in range(4):
+            disp = disp + jnp.where(info[k : k + 1] == here, 1.0, 0.0)
+        disp = disp[:, :64].astype(jnp.bfloat16)
+        data = jnp.concatenate([toks[zz, 0], toks[zz, 1]], axis=0)
+        for cut in range(2):
+            cols = slice(cut * 1024, cut * 1024 + 1024)
+            msgs[zz, :, :, cols] = (
+                jnp.dot(disp, data[:, cols], preferred_element_type=jnp.float32).astype(jnp.bfloat16).reshape(4, 8, 1024)
+            )
+        rows[t, zz * NX + x] = msgs[zz, x]
+        for i, dx in enumerate((1, 3, 2)):
+            to = lax.rem(x + dx, NX)
+            remote(
+                msgs.at[zz, to], rows.at[t, zz * NX + x], msend.at[dz * 3 + i], mrecv.at[zz * NX + x], plane(chip_at(0, dx))
+            ).start()
 
     def chunk_at(which, dz):
         first = lax.rem(z + NZ - dz, NZ) * NX
@@ -444,15 +416,22 @@
         if dz in VIA_DN:
             hand(t_up, dz, dn).start()
 
-    for i, dz in enumerate(GROUP_ORDER):
-        for dx in (0, 1, 3, 2):
-            if (dz, dx) != (0, 0):
-                source = chip_at(NZ - dz, dx)
-                remote(msgs.at[0], rows.at[t, source], msend.at[0], mrecv.at[source], partner).wait_recv()
+    def spread(dz):
+        zz = lax.rem(z + NZ - dz, NZ)
+        for dx in (1, 3, 2):
+            source = zz * NX + lax.rem(x + dx, NX)
+            remote(msgs.at[0, 0], rows.at[t, source], msend.at[0], mrecv.at[source], partner).wait_recv()
         give(dz, gup.at[dz], up).start()
         give(dz, gdn.at[dz], dn).start()
+
+    for i, dz in enumerate(GROUP_ORDER):
+        tokens_of(dz)
         if i > 0:
-            relay(GROUP_ORDER[i - 1])
+            spread(GROUP_ORDER[i - 1])
+        if i > 1:
+            relay(GROUP_ORDER[i - 2])
+    spread(GROUP_ORDER[7])
+    relay(GROUP_ORDER[6])
     for load in loads:
         load.wait()
 
@@ -530,7 +509,12 @@
     for dz, dx in others:
         source = chip_at(dz, dx)
         remote(part.at[t, 0], ret.at[source], rsend.at[0], rrecv.at[source], partner).wait_recv()
-    weight = mixw_ref[...]
+    info = infos[z, 0] + infos[z, 1]
+    everywhere = wanted(256, 0)
+    weight = jnp.zeros((256, 128), jnp.float32)
+    for k in range(4):
+        weight = weight + jnp.where(info[k : k + 1] == everywhere, info[4 + k : 5 + k], 0.0)
+    weight = weight.T[:64]
     coarse = weight.astype(jnp.bfloat16)
     fine = (weight - coarse.astype(jnp.float32)).astype(jnp.bfloat16)
     for cut in range(4):
@@ -545,12 +529,17 @@
     swap_mix.start()
 
     def sent(src, sem):
-        remote(src, src, sem, nsem.at[1], partner).wait_send()
+        remote(src, src, sem, xsem.at[1], partner).wait_send()
+
+    for i in range(15):
+        sent(toks.at[0, 0], tsend.at[i])
+        sent(infos.at[0, 0], isend.at[i])
+    for i in range(24):
+        sent(msgs.at[0, 0], msend.at[i])
 
     for dz, dx in others:
         to = chip_at(dz, dx)
-        sent(msgs.at[0], msend.at[to])
-        sent(msgs.at[0], rsend.at[to])
+        sent(msgs.at[0, 0], rsend.at[to])
     for i in range(8):
         for sems in (gup, gdn, gfw, s_first, s_direct, s_mid):
             sent(mid.at[0, 0], sems.at[i])
@@ -560,48 +549,81 @@
     out_ref[...] = (middle_ref[...] + mixture * scale * gain_ref[...]).astype(jnp.bfloat16)
 
 
-def experts(normed, disp, mixw, middle, gain, w_gate, w_up, w_down):
-    whole, remote = pl.BlockSpec(memory_space=pltpu.VMEM), pl.BlockSpec(memory_space=pl.ANY)
-    dma = pltpu.SemaphoreType.DMA
+ATTENTION_ITEMS = 25
+
+
+def layer_kernel(q_ref, kv_ref, wo_hbm, residual_ref, mix_ref, pre_ref, info_ref, gain_ref, wg_hbm, wu_hbm, wd_hbm, out_ref, *rest):
+    middle, normed, wsem = rest[:3]
+    attention_items = rest[3 : 3 + ATTENTION_ITEMS]
+    expert_items = rest[3 + ATTENTION_ITEMS :]
+    wg, wu, wd = expert_items[10:13]
+    sp = lax.axis_index("sp")
+    t = lax.axis_index("tp")
+    core = lax.rem(sp, 2)
+    chip = lax.div(sp, 2)
+    x = lax.rem(chip, NX)
+    z = lax.div(chip, NX)
+
+    def chip_at(dz, dx):
+        return lax.rem(z + dz, NZ) * NX + lax.rem(x + dx, NX)
+
+    others = [(dz, dx) for dz in GROUP_ORDER for dx in (0, 1, 3, 2) if (dz, dx) != (0, 0)]
+    column = [chip_at(dz, 0) * 2 + 1 - core for dz in range(1, NZ)]
+    loads = [pltpu.make_async_copy(src, dst, wsem.at[i]) for i, (src, dst) in enumerate(((wg_hbm, wg), (wu_hbm, wu), (wd_hbm, wd)))]
+
+    def meet():
+        barrier = pltpu.get_barrier_semaphore()
+        peers = [{"sp": chip * 2 + 1 - core}] + [{"tp": lax.rem(t + d, 4)} for d in (1, 2, 3)]
+        peers += [{"sp": chip_at(dz, dx) * 2 + core} for dz, dx in others] + [{"sp": to} for to in column]
+        for peer in peers:
+            pl.semaphore_signal(barrier, inc=1, device_id=peer, device_id_type=MESH)
+        pl.semaphore_wait(barrier, len(peers))
+
+    for load in loads:
+        load.start()
+    attention_part(q_ref, kv_ref, wo_hbm, residual_ref, mix_ref, pre_ref, middle, normed, meet, *attention_items)
+    experts_part(normed, info_ref, middle, gain_ref, loads, out_ref, others, column, *expert_items)
+
+
+def layer(q_two, kv_two, w_out, residual, gain_mix, gain_pre, info, gain_moe, w_gate, w_up, w_down):
+    whole, apart = pl.BlockSpec(memory_space=pltpu.VMEM), pl.BlockSpec(memory_space=pltpu.MemorySpace.HBM)
+    dma, bf16, f32 = pltpu.SemaphoreType.DMA, jnp.bfloat16, jnp.float32
+    attention_scratch = [
+        pltpu.VMEM((64, 2, PIECE, 128), bf16),
+        pltpu.VMEM((1024, 128), bf16),
+        pltpu.VMEM((1, 1024), f32),
+        pltpu.VMEM((1, 1024), f32),
+        pltpu.VMEM((128, 1024), f32),
+        pltpu.VMEM((3, 128, 512), bf16),
+        pltpu.VMEM((128, 1024), bf16),
+        pltpu.VMEM((1024, 2048), bf16),
+        pltpu.VMEM((4, 32, 2048), bf16),
+        pltpu.VMEM((3, 32, 2048), bf16),
+    ] + [dma((n,)) if n else dma for n in (64, 0, 3, 16, 16, 4, 4, 8, 8, 8, 2, 2, 3, 3, 0)]
+    expert_scratch = [
+        pltpu.VMEM((8, 2, 32, 2048), bf16),
+        pltpu.VMEM((8, 2, 8, 128), f32),
+        pltpu.VMEM((8, 4, 8, 2048), bf16),
+        pltpu.VMEM((4, 32, 8, 2048), bf16),
+        pltpu.VMEM((256, 512), bf16),
+        pltpu.VMEM((4, 32, 8, 2048), bf16),
+        pltpu.VMEM((2, 4, 4, 8, 2048), bf16),
+        pltpu.VMEM((2, 32, 8, 2048), bf16),
+        pltpu.VMEM((32, 8, 2048), bf16),
+        pltpu.VMEM((3, 32, 2048), f32),
+        pltpu.VMEM((2048, 512), bf16),
+        pltpu.VMEM((2048, 512), bf16),
+        pltpu.VMEM((512, 2048), bf16),
+    ] + [dma((n,)) for n in (15, 16, 15, 16, 24, 32, 8, 8, 8, 32, 8, 8, 8, 8, 16, 32, 32, 2)]
     return pl.pallas_call(
-        experts_kernel,
-        out_shape=jax.ShapeDtypeStruct((32, 2048), jnp.bfloat16),
-        in_specs=[whole] * 5 + [remote] * 3,
+        layer_kernel,
+        out_shape=jax.ShapeDtypeStruct((32, 2048), bf16),
+        in_specs=[whole, whole, apart, whole, whole, whole, whole, whole, apart, apart, apart],
         out_specs=whole,
-        scratch_shapes=[
-            pltpu.VMEM((2, 32, 2048), jnp.bfloat16),
-            pltpu.VMEM((32, 8, 2048), jnp.bfloat16),
-            pltpu.VMEM((4, 32, 8, 2048), jnp.bfloat16),
-            pltpu.VMEM((256, 512), jnp.bfloat16),
-            pltpu.VMEM((4, 32, 8, 2048), jnp.bfloat16),
-            pltpu.VMEM((2, 4, 4, 8, 2048), jnp.bfloat16),
-            pltpu.VMEM((2, 32, 8, 2048), jnp.bfloat16),
-            pltpu.VMEM((32, 8, 2048), jnp.bfloat16),
-            pltpu.VMEM((3, 32, 2048), jnp.float32),
-            pltpu.VMEM((2048, 512), jnp.bfloat16),
-            pltpu.VMEM((2048, 512), jnp.bfloat16),
-            pltpu.VMEM((512, 2048), jnp.bfloat16),
-            dma((3,)),
-            dma((32,)),
-            dma((32,)),
-            dma((8,)),
-            dma((8,)),
-            dma((8,)),
-            dma((32,)),
-            dma((8,)),
-            dma((8,)),
-            dma((8,)),
-            dma((8,)),
-            dma((16,)),
-            dma((32,)),
-            dma((32,)),
-            dma((2,)),
-            dma((2,)),
-        ],
-        compiler_params=pltpu.CompilerParams(collective_id=1, has_side_effects=True, vmem_limit_bytes=48 << 20),
-        cost_estimate=pl.CostEstimate(flops=6 * 1024 * 2048 * 512, bytes_accessed=8 << 20, transcendentals=1024 * 512),
-        name="experts",
-    )(normed, disp, mixw, middle, gain, w_gate, w_up, w_down)
+        scratch_shapes=[pltpu.VMEM((32, 2048), f32), pltpu.VMEM((32, 2048), bf16), dma((3,))] + attention_scratch + expert_scratch,
+        compiler_params=pltpu.CompilerParams(collective_id=0, has_side_effects=True, vmem_limit_bytes=58 << 20),
+        name="layer",
+    )(q_two, kv_two, w_out, residual, gain_mix, gain_pre, info, gain_moe, w_gate, w_up, w_down)
 
 
 def on_device(
@@ -636,12 +658,19 @@
     q_two = q_turned.transpose(1, 0, 2).reshape(kv_local, group_size * tok_rows, head_size)
     kv_two = jnp.stack([k_turned.transpose(1, 0, 2), values.transpose(1, 2, 0)], axis=1)
     width = residual.shape[1]
-    middle, normed = attention(
-        q_two, kv_two, w_out, residual, gain_mix.reshape(1, width), gain_pre.reshape(1, width)
-    )
-    disp, mixw = slot_tables(routes, route_weights)
-    return experts(
-        normed, disp, mixw, middle, gain_moe.reshape(1, width), w_gate[0], w_up[0], w_down[0]
+    info = route_info(routes, route_weights)
+    return layer(
+        q_two,
+        kv_two,
+        w_out,
+        residual,
+        gain_mix.reshape(1, width),
+        gain_pre.reshape(1, width),
+        info,
+        gain_moe.reshape(1, width),
+        w_gate[0],
+        w_up[0],
+        w_down[0],
     )
 
 

time: 169 us -> 166 us (0.982)
  starting transfers between devices: 3.2 us -> 0 us
  Pallas kernels: 155 us -> 158 us
  local copies, waits for them, and re-layouts: 6.79 us -> 4.57 us
    pallas_call x2 -> x1, Pallas kernels: 155 us -> 158 us  [layer(): pl.pallas_call(layer_kernel, out_shape=jax.ShapeDtypeStruct((32, 2048), b...]
    ppermute x1 -> x0, starting transfers between devices: 3.2 us -> none  [slot_tables(): other = lax.ppermute(both, 'sp', swap)]
    unnamed x24 -> x15, local copies, waits for them, and re-layouts: 5.87 us -> 3.08 us
  transfers between devices with their start and end apart: 1 -> 0, of which waited for: 0 -> 0; matrix products, arithmetic and copies ran while one was open for 2% -> 0% of each run, Pallas kernels for 34% -> 0%
where the time goes in v4:
time: 166 us
  Pallas kernels  158 us (95%)
  local copies, waits for them, and re-layouts  4.57 us (3%)
  other arithmetic  2.85 us (2%)
    pallas_call x1, Pallas kernels, layer(): pl.pallas_call(layer_kernel, out_shape=jax.ShapeDtypeStruct((32, 2048), b...  158 us

profile of v4, /device:TPU:1, one launch (start us, length us, event | category | flops | bytes accessed | tf_op | source)
XLA Modules:
  0.0 165.8 jit_solution(1461885635091233483)
XLA Ops:
  0.0 0.1 broadcast_multiply_fusion.1
  0.1 0.1 fusion.7
  0.2 0.0 copy-start.4
  0.3 1.2 copy.53
  1.4 0.1 fusion
  1.5 0.0 copy-start.1
  1.5 0.0 copy-start.2
  1.5 0.8 fusion.1
  2.3 0.0 copy-start.3
  2.3 0.1 multiply_subtract_fusion
  2.4 0.1 fusion.2
  2.5 0.8 copy.54
  3.3 0.0 copy-done
  3.3 0.1 copy.55
  3.5 0.0 copy-done.4
  3.5 0.1 fusion.4
  3.6 0.1 copy.56
  3.8 0.0 copy-done.1
  3.8 0.1 copy.57
  3.9 0.7 pad_maximum_fusion.kv_ref
  4.6 0.1 broadcast_in_dim.19
  4.6 0.1 broadcast_in_dim.20
  4.7 0.0 copy-done.2
  4.7 0.1 copy.58
  4.8 0.1 eq.30
  4.9 0.2 convert_reduce_fusion
  5.1 0.1 reduce_sum.32
  5.2 0.1 copy.59
  5.3 0.1 broadcast_in_dim.46
  5.4 0.6 broadcast_select_fusion.info_ref
  6.0 158.2 %layer.1 = bf16[32,2048]{1,0:T(8,128)(2,1)} custom-call(bf16[2,512,128]{2,1,0:T(8,128)(2,1)} %bitcast.26, bf16[2,2,128,128]{3,2,1,0:T(8,128)(2,1)} %pad_maximum_fusion.kv_ref, bf16[1024,2048]{1,0:T(8,128)(2,1)} %wo_hbm.1, bf16[32,2048]{1,0:T(8,128)(2,1)} %residual_ref.1, f32[1,2048]{1,0:T(1,128)} %bitcast.32, f32[1,2048]{1,0:T(1,128)} %bitcast.33, ...), custom_call_target="tpu_custom_call" | custom-call | tf_op jit(solution)/shard_map/layer/pallas_call | solution.py:618
  164.2 1.6 copy.61
  (13 shorter events, 0.1 us)
Async XLA Ops:
  0.0 3.3 %copy-start = (bf16[128,2,128]{2,1,0:T(2,128)(2,1)S(1)}, bf16[128,2,128]{2,1,0:T(2,128)(2,1)}, u32[]{:S(2)}) copy-start(bf16[128,2,128]{2,1,0:T(2,128)(2,1)} %param.16) | copy-start | bytes 196612
  0.2 3.2 %copy-start.4 = (f32[128]{0:T(128)S(1)}, f32[128]{0:T(128)}, u32[]{:S(2)}) copy-start(f32[128]{0:T(128)} %param.19) | copy-start | bytes 1540
  1.5 2.3 %copy-start.1 = (bf16[128,2,128]{2,1,0:T(2,128)(2,1)S(1)}, bf16[128,2,128]{2,1,0:T(2,128)(2,1)}, u32[]{:S(2)}) copy-start(bf16[128,2,128]{2,1,0:T(2,128)(2,1)} %param.17) | copy-start | bytes 196612
  1.5 3.2 %copy-start.2 = (s32[32,4]{0,1:T(4,128)S(1)}, s32[32,4]{0,1:T(4,128)}, u32[]{:S(2)}) copy-start(s32[32,4]{0,1:T(4,128)} %param.24) | copy-start | bytes 1540
  2.3 3.0 %copy-start.3 = (f32[32,4]{0,1:T(4,128)S(1)}, f32[32,4]{0,1:T(4,128)}, u32[]{:S(2)}) copy-start(f32[32,4]{0,1:T(4,128)} %param.25) | copy-start | bytes 1540

commit v5 on v4

--- a/solution.py
+++ b/solution.py
@@ -213,31 +213,73 @@
             arrive(at)
             ready.append(at)
 
+    swap_q.wait_recv()
     lines_a(0, 1)
+    work()
     lines_a(0, 3)
+    work()
     lines_a(0, 2)
-    swap_q.wait_recv()
-    for r in range(1, 5):
-        lines_b(r)
-        work()
-        lines_a(r, 0)
-        work()
-        lines_a(r, 1)
-        work()
-        across(r - 1)
-        work()
-        lines_a(r, 3)
-        work()
-        lines_a(r, 2)
-        work()
-        if r > 1:
-            far(r - 2)
-        work()
+    work()
+    lines_b(1)
+    work()
+    lines_a(1, 0)
+    work()
+    lines_a(1, 1)
+    work()
+    across(0)
+    work()
+    lines_b(2)
+    work()
+    lines_a(1, 3)
+    work()
+    lines_a(1, 2)
+    work()
+    across(1)
+    work()
+    far(0)
+    work()
+    lines_a(2, 0)
+    work()
+    lines_a(2, 1)
+    work()
+    lines_b(3)
+    work()
+    across(2)
+    work()
+    far(1)
+    work()
+    lines_a(2, 3)
+    work()
+    lines_a(2, 2)
+    work()
+    lines_b(4)
+    work()
+    lines_a(3, 0)
+    work()
+    lines_a(3, 1)
+    work()
+    across(3)
+    work()
+    far(2)
+    work()
+    lines_a(3, 3)
+    work()
+    lines_a(3, 2)
+    work()
     across(4)
     work()
     far(3)
     work()
+    lines_a(4, 0)
+    work()
+    lines_a(4, 1)
+    work()
     far(4)
+    work()
+    lines_a(4, 3)
+    work()
+    lines_a(4, 2)
+    work()
     while ready:
         work(1)
 
@@ -424,14 +466,13 @@
         give(dz, gup.at[dz], up).start()
         give(dz, gdn.at[dz], dn).start()
 
-    for i, dz in enumerate(GROUP_ORDER):
-        tokens_of(dz)
-        if i > 0:
+    for i in range(11):
+        if i < 8:
+            tokens_of(GROUP_ORDER[i])
+        if 1 <= i < 9:
             spread(GROUP_ORDER[i - 1])
-        if i > 1:
-            relay(GROUP_ORDER[i - 2])
-    spread(GROUP_ORDER[7])
-    relay(GROUP_ORDER[6])
+        if i >= 4:
+            relay(GROUP_ORDER[i - 4])
     for load in loads:
         load.wait()
 
@@ -487,21 +528,21 @@
     serve(t_up)
     serve(t_dn)
     direct(0)
+    direct(1)
     for dz in GROUP_ORDER:
         take(t_far, dz)
     serve(t_far)
     first(0)
     first(1)
     middle_sum(0)
-    direct(1)
     first(2)
     middle_sum(1)
+    direct(2)
     settle(0)
-    direct(2)
     first(3)
     middle_sum(2)
+    direct(3)
     settle(1)
-    direct(3)
     middle_sum(3)
     settle(2)
     settle(3)
@@ -621,7 +662,7 @@
         in_specs=[whole, whole, apart, whole, whole, whole, whole, whole, apart, apart, apart],
         out_specs=whole,
         scratch_shapes=[pltpu.VMEM((32, 2048), f32), pltpu.VMEM((32, 2048), bf16), dma((3,))] + attention_scratch + expert_scratch,
-        compiler_params=pltpu.CompilerParams(collective_id=0, has_side_effects=True, vmem_limit_bytes=58 << 20),
+        compiler_params=pltpu.CompilerParams(collective_id=0, has_side_effects=True, vmem_limit_bytes=40 << 20),
         name="layer",
     )(q_two, kv_two, w_out, residual, gain_mix, gain_pre, info, gain_moe, w_gate, w_up, w_down)
 

time: 166 us -> 161 us (0.970)
  Pallas kernels: 158 us -> 150 us
  local copies, waits for them, and re-layouts: 4.57 us -> 8.4 us
    pallas_call x1, Pallas kernels: 158 us -> 150 us  [layer(): pl.pallas_call(layer_kernel, out_shape=jax.ShapeDtypeStruct((32, 2048), b...]
    unnamed x15 -> x31, local copies, waits for them, and re-layouts: 3.08 us -> 7.57 us
where the time goes in v5:
time: 161 us
  Pallas kernels  150 us (93%)
  local copies, waits for them, and re-layouts  8.4 us (5%)
    pallas_call x1, Pallas kernels, layer(): pl.pallas_call(layer_kernel, out_shape=jax.ShapeDtypeStruct((32, 2048), b...  150 us
    unnamed x31, local copies, waits for them, and re-layouts  7.57 us

profile of v5, /device:TPU:1, one launch (start us, length us, event | category | flops | bytes accessed | tf_op | source)
XLA Modules:
  0.0 160.6 jit_solution(13097923314810351403)
XLA Ops:
  0.0 0.1 broadcast_multiply_fusion.1
  0.1 0.1 fusion.7
  0.2 0.0 copy-start.12
  0.3 1.2 copy.53
  1.4 0.1 fusion
  1.5 0.0 copy-start.9
  1.5 0.0 copy-start.10
  1.5 0.8 fusion.1
  2.3 0.0 copy-start.11
  2.3 0.0 copy-start.1
  2.3 0.0 copy-start.4
  2.4 0.0 copy-start.7
  2.4 0.1 multiply_subtract_fusion
  2.4 0.1 fusion.2
  2.5 0.2 copy.54
  2.7 0.1 copy.55
  2.9 0.1 fusion.4
  3.0 0.1 copy.56
  3.2 0.1 copy.57
  3.3 0.1 broadcast_in_dim.19
  3.4 0.1 broadcast_in_dim.20
  3.5 0.1 copy.58
  3.6 0.1 eq.30
  3.7 0.2 convert_reduce_fusion
  3.9 0.1 reduce_sum.32
  4.0 0.1 copy.59
  4.1 0.1 broadcast_in_dim.46
  4.3 2.2 %copy-done = bf16[1024,2048]{1,0:T(8,128)(2,1)S(1)} copy-done((bf16[1024,2048]{1,0:T(8,128)(2,1)S(1)}, bf16[1024,2048]{1,0:T(8,128)(2,1)}, u32[]{:S(2)}) %copy-start) | copy-done | bytes 4194328
  6.4 1.6 copy-done.2
  8.0 1.6 copy-done.3
  9.6 150.4 %layer.1 = bf16[32,2048]{1,0:T(8,128)(2,1)S(1)} custom-call(bf16[2,512,128]{2,1,0:T(8,128)(2,1)S(1)} %bitcast.25, bf16[2,2,128,128]{3,2,1,0:T(8,128)(2,1)S(1)} %pad_maximum_fusion.kv_ref, bf16[1024,2048]{1,0:T(8,128)(2,1)S(1)} %copy-done, bf16[32,2048]{1,0:T(8,128)(2,1)S(1)} %copy-done.4, f32[1,2048]{1,0:T(1,128)S(1)} %bitcast.26, f32[1,2048]{1,0:T(1,128)S(1)} %bitcast.27, ...), custom_call_target="tpu_custom_call" | custom-call | tf_op jit(solution)/shard_map/layer/pallas_call | solution.py:659
  160.0 0.7 copy.61
  (29 shorter events, 0.2 us)
Async XLA Ops:
  0.0 2.7 %copy-start.8 = (bf16[128,2,128]{2,1,0:T(2,128)(2,1)S(1)}, bf16[128,2,128]{2,1,0:T(2,128)(2,1)}, u32[]{:S(2)}) copy-start(bf16[128,2,128]{2,1,0:T(2,128)(2,1)} %param.16) | copy-start | bytes 196612
  0.2 2.7 %copy-start.12 = (f32[128]{0:T(128)S(1)}, f32[128]{0:T(128)}, u32[]{:S(2)}) copy-start(f32[128]{0:T(128)} %param.19) | copy-start | bytes 1540
  1.5 1.7 %copy-start.9 = (bf16[128,2,128]{2,1,0:T(2,128)(2,1)S(1)}, bf16[128,2,128]{2,1,0:T(2,128)(2,1)}, u32[]{:S(2)}) copy-start(bf16[128,2,128]{2,1,0:T(2,128)(2,1)} %param.17) | copy-start | bytes 196612
  1.5 2.0 %copy-start.10 = (s32[32,4]{0,1:T(4,128)S(1)}, s32[32,4]{0,1:T(4,128)}, u32[]{:S(2)}) copy-start(s32[32,4]{0,1:T(4,128)} %param.24) | copy-start | bytes 1540
  2.3 1.8 %copy-start.11 = (f32[32,4]{0,1:T(4,128)S(1)}, f32[32,4]{0,1:T(4,128)}, u32[]{:S(2)}) copy-start(f32[32,4]{0,1:T(4,128)} %param.25) | copy-start | bytes 1540
  2.3 1.9 %copy-start.1 = (bf16[1,2048,512]{2,1,0:T(8,128)(2,1)S(1)}, bf16[1,2048,512]{2,1,0:T(8,128)(2,1)}, u32[]{:S(2)}) copy-start(bf16[1,2048,512]{2,1,0:T(8,128)(2,1)} %param.26) | copy-start | bytes 6291460
  2.3 1.9 %copy-start.4 = (bf16[32,2048]{1,0:T(8,128)(2,1)S(1)}, bf16[32,2048]{1,0:T(8,128)(2,1)}, u32[]{:S(2)}) copy-start(bf16[32,2048]{1,0:T(8,128)(2,1)} %residual_ref.1) | copy-start | bytes 393220
  2.3 1.9 %copy-start.5 = (f32[2048]{0:T(1024)S(1)}, f32[2048]{0:T(1024)}, u32[]{:S(2)}) copy-start(f32[2048]{0:T(1024)} %param.22) | copy-start | bytes 24580
  2.3 1.9 %copy-start.6 = (f32[2048]{0:T(1024)S(1)}, f32[2048]{0:T(1024)}, u32[]{:S(2)}) copy-start(f32[2048]{0:T(1024)} %param.23) | copy-start | bytes 24580
  2.4 1.9 %copy-start.7 = (f32[2048]{0:T(1024)S(1)}, f32[2048]{0:T(1024)}, u32[]{:S(2)}) copy-start(f32[2048]{0:T(1024)} %param.29) | copy-start | bytes 24580
  4.2 2.2 %copy-start = (bf16[1024,2048]{1,0:T(8,128)(2,1)S(1)}, bf16[1024,2048]{1,0:T(8,128)(2,1)}, u32[]{:S(2)}) copy-start(bf16[1024,2048]{1,0:T(8,128)(2,1)} %wo_hbm.1) | copy-start | bytes 12582916
  6.4 1.6 copy-start.2
  8.0 1.6 copy-start.3

commit v6 on v5

--- a/solution.py
+++ b/solution.py
@@ -24,42 +24,12 @@
     return (jnp.cos(angles), jnp.sin(angles))
 
 
-def turn(array_in, cosine_table, sine_table):
-    token_count, head_count, head_size = array_in.shape
-    split_field = array_in.reshape(token_count, head_count, 2, 2, head_size // 4)
-    first_half = split_field[:, :, :, 0, :]
-    second_half = split_field[:, :, :, 1, :]
-    cos_wide = cosine_table[:, None]
-    sin_wide = sine_table[:, None]
-    turned = jnp.stack(
-        [
-            first_half * cos_wide - second_half * sin_wide,
-            second_half * cos_wide + first_half * sin_wide,
-        ],
-        axis=3,
-    )
-    return turned.reshape(token_count, head_count, head_size)
-
-
 def scale_rows(array_in, gain_vec):
     return (
         array_in
         * lax.rsqrt(jnp.mean(array_in * array_in, axis=-1, keepdims=True) + norm_eps)
         * gain_vec
     )
-
-
-def route_info(routes, route_weights):
-    core = lax.rem(lax.axis_index("sp"), 2)
-    count = routes.shape[0]
-    flat = routes.reshape(-1)
-    place = jnp.arange(count * TOP, dtype=jnp.int32)
-    earlier = (flat[:, None] == flat[None, :]) & (place[None, :] < place[:, None])
-    rank = jnp.sum(earlier.astype(jnp.int32), axis=1)
-    slots = (flat * 4 + rank).reshape(count, TOP).astype(jnp.float32)
-    info = jnp.concatenate([slots.T, route_weights.T], axis=0)
-    side = jnp.arange(128 // count, dtype=jnp.int32)[None, :, None]
-    return jnp.where(side == core, info[:, None, :], 0.0).reshape(2 * TOP, 128)
 
 
 MESH = pl.DeviceIdType.MESH
@@ -593,10 +563,48 @@
 ATTENTION_ITEMS = 25
 
 
-def layer_kernel(q_ref, kv_ref, wo_hbm, residual_ref, mix_ref, pre_ref, info_ref, gain_ref, wg_hbm, wu_hbm, wd_hbm, out_ref, *rest):
-    middle, normed, wsem = rest[:3]
-    attention_items = rest[3 : 3 + ATTENTION_ITEMS]
-    expert_items = rest[3 + ATTENTION_ITEMS :]
+def prepare(q_raw, k_raw, v_turned, table_ref, qgain_ref, kgain_ref, q_wide, k_wide, q_two, kv_two):
+    cosine, sine = table_ref[0], table_ref[1]
+    second = (lax.broadcasted_iota(jnp.int32, (128, 128), 1) // 32) % 2 == 1
+
+    def turned(rows, gain):
+        scaled = scale_rows(rows, gain)
+        other = jnp.where(second, pltpu.roll(scaled, 32, 1), pltpu.roll(scaled, 96, 1))
+        return scaled * cosine + other * sine
+
+    k_wide[...] = k_raw[...].astype(jnp.float32)
+    q_wide[...] = q_raw[...].astype(jnp.float32)
+    for g in range(2):
+        kv_two[g, 0] = turned(k_wide[pl.ds(g, 128, stride=2), :], kgain_ref[...]).astype(jnp.bfloat16)
+        kv_two[g, 1] = v_turned[g]
+        for h in range(4):
+            rows = q_wide[pl.ds(g * 4 + h, 128, stride=8), :]
+            q_two[g, h * 128 : h * 128 + 128, :] = (turned(rows, qgain_ref[...]) * 128 ** (-0.5)).astype(jnp.bfloat16)
+
+
+def fill_info(routes_ref, lists_ref, info, core):
+    chosen = routes_ref[...].astype(jnp.float32)
+    lists = lists_ref[...]
+    row = lax.broadcasted_iota(jnp.int32, (32, 128), 0)
+    lane = lax.broadcasted_iota(jnp.int32, (32, 128), 1)
+    before = row < lane
+    slots = []
+    for k in range(4):
+        rank = jnp.zeros((1, 128), jnp.float32)
+        for other in range(4):
+            same = (chosen[:, other : other + 1] == lists[k : k + 1]) & before
+            rank = rank + jnp.sum(jnp.where(same, 1.0, 0.0), axis=0, keepdims=True)
+        slots.append(lists[k : k + 1] * 4.0 + rank)
+    both = jnp.concatenate(slots + [lists[4:]], axis=0)
+    both = jnp.where(lax.broadcasted_iota(jnp.int32, (8, 128), 1) < 32, both, 0.0)
+    info[...] = jnp.where(core == 0, both, pltpu.roll(both, 32, 1))
+
+
+def layer_kernel(q_raw, k_raw, v_turned, table_ref, qgain_ref, kgain_ref, routes_ref, lists_ref, wo_hbm, residual_ref, mix_ref,
+                 pre_ref, gain_ref, wg_hbm, wu_hbm, wd_hbm, out_ref, *rest):
+    middle, normed, wsem, q_wide, k_wide, q_ref, kv_ref, info_ref = rest[:8]
+    attention_items = rest[8 : 8 + ATTENTION_ITEMS]
+    expert_items = rest[8 + ATTENTION_ITEMS :]
     wg, wu, wd = expert_items[10:13]
     sp = lax.axis_index("sp")
     t = lax.axis_index("tp")
@@ -622,11 +630,13 @@
 
     for load in loads:
         load.start()
+    prepare(q_raw, k_raw, v_turned, table_ref, qgain_ref, kgain_ref, q_wide, k_wide, q_ref, kv_ref)
+    fill_info(routes_ref, lists_ref, info_ref, core)
     attention_part(q_ref, kv_ref, wo_hbm, residual_ref, mix_ref, pre_ref, middle, normed, meet, *attention_items)
     experts_part(normed, info_ref, middle, gain_ref, loads, out_ref, others, column, *expert_items)
 
 
-def layer(q_two, kv_two, w_out, residual, gain_mix, gain_pre, info, gain_moe, w_gate, w_up, w_down):
+def layer(queries, keys, values, tables, q_gain, k_gain, routes, lists, w_out, residual, gain_mix, gain_pre, gain_moe, w_gate, w_up, w_down):
     whole, apart = pl.BlockSpec(memory_space=pltpu.VMEM), pl.BlockSpec(memory_space=pltpu.MemorySpace.HBM)
     dma, bf16, f32 = pltpu.SemaphoreType.DMA, jnp.bfloat16, jnp.float32
     attention_scratch = [
@@ -659,12 +669,23 @@
     return pl.pallas_call(
         layer_kernel,
         out_shape=jax.ShapeDtypeStruct((32, 2048), bf16),
-        in_specs=[whole, whole, apart, whole, whole, whole, whole, whole, apart, apart, apart],
+        in_specs=[whole] * 8 + [apart] + [whole] * 4 + [apart] * 3,
         out_specs=whole,
-        scratch_shapes=[pltpu.VMEM((32, 2048), f32), pltpu.VMEM((32, 2048), bf16), dma((3,))] + attention_scratch + expert_scratch,
-        compiler_params=pltpu.CompilerParams(collective_id=0, has_side_effects=True, vmem_limit_bytes=40 << 20),
+        scratch_shapes=[
+            pltpu.VMEM((32, 2048), f32),
+            pltpu.VMEM((32, 2048), bf16),
+            dma((3,)),
+            pltpu.VMEM((1024, 128), f32),
+            pltpu.VMEM((256, 128), f32),
+            pltpu.VMEM((2, 512, 128), bf16),
+            pltpu.VMEM((2, 2, 128, 128), bf16),
+            pltpu.VMEM((8, 128), f32),
+        ]
+        + attention_scratch
+        + expert_scratch,
+        compiler_params=pltpu.CompilerParams(collective_id=0, has_side_effects=True, vmem_limit_bytes=52 << 20),
         name="layer",
-    )(q_two, kv_two, w_out, residual, gain_mix, gain_pre, info, gain_moe, w_gate, w_up, w_down)
+    )(queries, keys, values, tables, q_gain, k_gain, routes, lists, w_out, residual, gain_mix, gain_pre, gain_moe, w_gate, w_up, w_down)
 
 
 def on_device(
@@ -686,28 +707,25 @@
 ):
     tok_rows, head_local, head_size = queries.shape
     kv_local = keys.shape[1]
-    group_size = head_local // kv_local
     positions = lax.axis_index("sp") * tok_rows + jnp.arange(tok_rows, dtype=jnp.int32)
     cosine_table, sine_table = rope_tables(positions, head_size)
-    q_turned = (
-        turn(scale_rows(queries.astype(jnp.float32), q_gain), cosine_table, sine_table)
-        * head_size ** (-0.5)
-    ).astype(jnp.bfloat16)
-    k_turned = turn(scale_rows(keys.astype(jnp.float32), k_gain), cosine_table, sine_table).astype(
-        jnp.bfloat16
-    )
-    q_two = q_turned.transpose(1, 0, 2).reshape(kv_local, group_size * tok_rows, head_size)
-    kv_two = jnp.stack([k_turned.transpose(1, 0, 2), values.transpose(1, 2, 0)], axis=1)
+    cosines = jnp.stack([cosine_table, cosine_table], axis=2).reshape(tok_rows, head_size)
+    sines = jnp.stack([-sine_table, sine_table], axis=2).reshape(tok_rows, head_size)
     width = residual.shape[1]
-    info = route_info(routes, route_weights)
+    lists = jnp.concatenate([routes.T.astype(jnp.float32), route_weights.T], axis=0)
     return layer(
-        q_two,
-        kv_two,
+        queries.reshape(tok_rows * head_local, head_size),
+        keys.reshape(tok_rows * kv_local, head_size),
+        values.transpose(1, 2, 0),
+        jnp.stack([cosines, sines]),
+        q_gain.reshape(1, head_size),
+        k_gain.reshape(1, head_size),
+        routes,
+        jnp.pad(lists, ((0, 0), (0, 128 - lists.shape[1]))),
         w_out,
         residual,
         gain_mix.reshape(1, width),
         gain_pre.reshape(1, width),
-        info,
         gain_moe.reshape(1, width),
         w_gate[0],
         w_up[0],

time: 161 us -> 162 us (level)
    unnamed x31 -> x19, local copies, waits for them, and re-layouts: 7.57 us -> 8.46 us
where the time goes in v6:
time: 162 us; the launch traced here: 161 us
  Pallas kernels  151 us (93%)
  local copies, waits for them, and re-layouts  8.64 us (5%)
  other arithmetic  1.62 us (1%)
    pallas_call x1, Pallas kernels, layer(): pl.pallas_call(layer_kernel, out_shape=jax.ShapeDtypeStruct((32, 2048), b...  151 us
    unnamed x19, local copies, waits for them, and re-layouts  8.46 us

profile of v6, /device:TPU:1, one launch (start us, length us, event | category | flops | bytes accessed | tf_op | source)
XLA Modules:
  0.0 161.5 jit_solution(12392855396436005212)
XLA Ops:
  0.0 0.7 convert_bitcast_fusion
  0.7 0.7 select_maximum_fusion.lists_ref
  1.4 0.8 copy.22.routes_ref
  2.2 0.1 multiply_bitcast_fusion.1
  2.2 1.0 copy.19
  3.2 0.1 fusion.1
  3.4 0.1 copy.20
  3.5 0.1 copy.21
  3.6 0.0 copy-start
  3.6 0.9 copy-done
  4.5 0.0 copy-start.1
  4.5 0.9 copy-done.1
  5.4 0.0 copy-start.2
  5.4 0.8 copy-done.2
  6.3 0.0 copy-start.3
  6.3 0.7 copy-done.3
  7.0 0.0 copy-start.4
  7.0 0.7 copy-done.4
  7.7 0.0 copy-start.5
  7.7 0.7 copy-done.5
  8.4 0.0 copy-start.6
  8.4 0.7 copy-done.6
  9.0 0.0 copy-start.7
  9.0 0.7 copy-done.7
  9.7 151.1 %layer.1 = bf16[32,2048]{1,0:T(8,128)(2,1)S(1)} custom-call(bf16[1024,128]{1,0:T(8,128)(2,1)S(1)} %bitcast.21, bf16[256,128]{1,0:T(8,128)(2,1)S(1)} %bitcast.22, bf16[2,128,128]{2,1,0:T(8,128)(2,1)S(1)} %bitcast.20, f32[2,128,128]{2,1,0:T(8,128)S(1)} %pad_maximum_fusion.table_ref, f32[1,128]{1,0:T(1,128)S(1)} %bitcast.26, f32[1,128]{1,0:T(1,128)S(1)} %bitcast.27, ...), custom_call_target="tpu_custom_call" | custom-call | tf_op jit(solution)/shard_map/layer/pallas_call | solution.py:669
  160.8 0.7 copy.24
  (5 shorter events, 0.0 us)
Async XLA Ops:
  3.6 1.0 copy-start
  4.5 0.9 copy-start.1
  5.4 0.8 copy-start.2
  6.3 0.7 copy-start.3
  7.0 0.7 copy-start.4
  7.7 0.7 copy-start.5
  8.4 0.7 copy-start.6
  9.0 0.7 copy-start.7

commit v7 on v6

--- a/solution.py
+++ b/solution.py
@@ -683,7 +683,7 @@
         ]
         + attention_scratch
         + expert_scratch,
-        compiler_params=pltpu.CompilerParams(collective_id=0, has_side_effects=True, vmem_limit_bytes=52 << 20),
+        compiler_params=pltpu.CompilerParams(collective_id=0, has_side_effects=True, vmem_limit_bytes=54 << 20),
         name="layer",
     )(queries, keys, values, tables, q_gain, k_gain, routes, lists, w_out, residual, gain_mix, gain_pre, gain_moe, w_gate, w_up, w_down)
 

time: 162 us -> 161 us (level)
  local copies, waits for them, and re-layouts: 8.64 us -> 4.68 us
  Pallas kernels: 151 us -> 153 us
    unnamed x19 -> x3, local copies, waits for them, and re-layouts: 8.46 us -> 4.5 us
    pallas_call x1, Pallas kernels: 151 us -> 153 us  [layer(): pl.pallas_call(layer_kernel, out_shape=jax.ShapeDtypeStruct((32, 2048), b...]
where the time goes in v7:
time: 161 us
  Pallas kernels  153 us (95%)
  local copies, waits for them, and re-layouts  4.68 us (3%)
  other arithmetic  2.87 us (2%)
    pallas_call x1, Pallas kernels, layer(): pl.pallas_call(layer_kernel, out_shape=jax.ShapeDtypeStruct((32, 2048), b...  153 us
    unnamed x3, local copies, waits for them, and re-layouts  4.5 us

profile of v7, /device:TPU:1, one launch (start us, length us, event | category | flops | bytes accessed | tf_op | source)
XLA Modules:
  0.0 160.5 jit_solution(11636630340858324011)
XLA Ops:
  0.0 0.7 convert_bitcast_fusion
  0.7 1.3 select_maximum_fusion.lists_ref
  2.0 1.4 copy.22.routes_ref
  3.4 0.1 multiply_bitcast_fusion.1
  3.4 1.6 copy.19
  5.0 0.1 fusion.1
  5.1 0.1 copy.20
  5.3 0.1 copy.21
  5.4 0.7 pad_maximum_fusion.table_ref
  6.0 152.9 %layer.1 = bf16[32,2048]{1,0:T(8,128)(2,1)} custom-call(bf16[1024,128]{1,0:T(8,128)(2,1)} %bitcast.24, bf16[256,128]{1,0:T(8,128)(2,1)} %bitcast.27, bf16[2,128,128]{2,1,0:T(8,128)(2,1)} %bitcast.23, f32[2,128,128]{2,1,0:T(8,128)} %pad_maximum_fusion.table_ref, f32[1,128]{1,0:T(1,128)} %bitcast.32, f32[1,128]{1,0:T(1,128)} %bitcast.33, ...), custom_call_target="tpu_custom_call" | custom-call | tf_op jit(solution)/shard_map/layer/pallas_call | solution.py:669
  159.0 1.6 copy.24
  (4 shorter events, 0.0 us)
